TPU v7x, 32 devices: a whole 2x2x4 slice. The times are simulated.
32 devices in a mesh: ep: 8 (over z, core), tp: 4 (over y, x).
Axes of the slice: x: 2, y: 2, z: 4, core: 2. Of those that a mesh axis runs over, the one named last changes fastest.
Arguments:
- tokens: bfloat16 [1024, 4096], P('ep', 'tp'), may hold values from -6 to 6
- routes: int32 [1024, 2], P('ep'), may hold values from 0 to 15, all different within a row; in each aligned block of 128 rows (0 to 127, 128 to 255, ...) at most 20 rows name the same one
- route_weights: float32 [1024, 2], P('ep'), may hold values from 0.2 to 2
- cotangent: bfloat16 [1024, 4096], P('ep', 'tp'), may hold values from -6 to 6
- expert_gate: bfloat16 [16, 4096, 512], P('ep', 'tp'), may hold values from -0.09375 to 0.09375
- expert_up: bfloat16 [16, 4096, 512], P('ep', 'tp'), may hold values from -0.09375 to 0.09375
- expert_down: bfloat16 [16, 512, 4096], P('ep', None, 'tp'), may hold values from -0.25 to 0.25
- shared_gate: bfloat16 [4096, 512], P('tp'), may hold values from -0.09375 to 0.09375
- shared_up: bfloat16 [4096, 512], P('tp'), may hold values from -0.09375 to 0.09375
- shared_down: bfloat16 [512, 4096], P(None, 'tp'), may hold values from -0.25 to 0.25
Outputs:
- grad_tokens: bfloat16 [1024, 4096], P('ep', 'tp')
- grad_weights: float32 [1024, 2], P('ep')
- grad_expert_gate: float32 [16, 4096, 512], P('ep', 'tp')
- grad_expert_up: float32 [16, 4096, 512], P('ep', 'tp')
- grad_expert_down: float32 [16, 512, 4096], P('ep', None, 'tp')
- grad_shared_gate: float32 [4096, 512], P('tp', 'ep')
- grad_shared_up: float32 [4096, 512], P('tp', 'ep')
- grad_shared_down: float32 [512, 4096], P('ep', 'tp')
Inputs may be any that keep to these rules, and one draw needn't show every extreme that they name: `routes`: each row names 2 different experts. In each aligned block of 128 rows (the rows of one index of ep) no expert is named by more than 20 rows, a bound that some block reaches.
All inputs are finite; a program needn't handle non-finite values.
Results may differ from a plain program's by a relative error of at most 0.0054.
Values may be sent and summed in bfloat16 or wider, within the bound.
A program may use at most 64 MiB of HBM per device.

v0:
```python
import functools

import jax
import jax.numpy as jnp
from jax import lax
from jax.experimental import pallas as pl
from jax.experimental.pallas import tpu as pltpu
from jax.sharding import PartitionSpec as P

CORES = 2
BF = jnp.bfloat16
F32 = jnp.float32


def up_to(value, unit):
    return -(-value // unit) * unit


def dot(a, b):
    return jnp.dot(a, b, preferred_element_type=F32)


def dot_t(a, b):
    return lax.dot_general(a, b, (((1,), (1,)), ((), ())), preferred_element_type=F32)


def hidden_terms(gate_pre, up_pre, back_grad, scaling):
    logistic = jax.nn.sigmoid(gate_pre)
    silu = gate_pre * logistic
    product = silu * up_pre
    grad_act = back_grad if scaling is None else scaling * back_grad
    gate_grad = grad_act * up_pre * logistic * (1.0 + gate_pre * (1.0 - logistic))
    hidden = product if scaling is None else scaling * product
    return (
        gate_grad.astype(BF),
        (grad_act * silu).astype(BF),
        hidden.astype(BF),
        jnp.sum(back_grad * product, axis=-1, keepdims=True),
    )


def ring_plan(length):
    plan = []
    for step in range(1, length // 2 + 1):
        last_even = length % 2 == 0 and step == length // 2
        plan.append((step, 0, (0,) if last_even else (0, 1)))
        plan.append((step, 1, (1,) if last_even else (1, 0)))
    return plan


def kernel(
    dims,
    meta_in,
    tok_in,
    cot_in,
    eg_in,
    eu_in,
    ed_in,
    sg_in,
    su_in,
    sd_in,
    gtok_out,
    gw_out,
    osg,
    osu,
    osd,
    stok,
    scot,
    hg,
    hu,
    hh,
    all_tok,
    all_cot,
    all_meta,
    eg,
    eu,
    ed,
    sg,
    su,
    sd,
    sel,
    gates,
    sh_part,
    sh_recv,
    sh_all,
    share_t,
    part,
    exact,
    recv,
    dgs,
    back_send,
    back,
    shsum,
    load_sem,
    own_sem,
    ring_s,
    ring_r,
    mate_s,
    mate_r,
    shr_s,
    shr_r,
    sha_s,
    sha_r,
    pr_s,
    pr_r,
    pa_s,
    pa_r,
    xt_s,
    xt_r,
    bk_s,
    bk_r,
):
    ep, tp, tok, dl, ne, ff, sff, cap, re, rows, rpp, rpt, cp, swid = dims
    me = lax.axis_index("ep")
    mt = lax.axis_index("tp")
    length = ep // CORES
    chip = me // CORES
    core = me % CORES
    mate = chip * CORES + (1 - core)
    nxt = ((chip + 1) % length) * CORES + core
    prv = ((chip + length - 1) % length) * CORES + core

    owns = []
    for n, (src, dst) in enumerate(((tok_in, all_tok), (cot_in, all_cot), (meta_in, all_meta))):
        c = pltpu.make_async_copy(src, dst.at[me], own_sem.at[n])
        c.start()
        owns.append(c)
    loads = []
    for n, (src, dst) in enumerate(
        ((sg_in, sg), (su_in, su), (sd_in, sd), (eg_in, eg), (eu_in, eu), (ed_in, ed))
    ):
        c = pltpu.make_async_copy(src, dst, load_sem.at[n])
        c.start()
        loads.append(c)

    barrier = pltpu.get_barrier_semaphore()
    for o in range(1, ep):
        pl.semaphore_signal(barrier, inc=1, device_id={"ep": (me + o) % ep})
    for o in range(1, tp):
        pl.semaphore_signal(barrier, inc=1, device_id={"tp": (mt + o) % tp})
    pl.semaphore_wait(barrier, ep + tp - 2)

    sends = []

    def remote(src, dst, ssem, rsem, dev):
        c = pltpu.make_async_remote_copy(
            src_ref=src, dst_ref=dst, send_sem=ssem, recv_sem=rsem, device_id=dev
        )
        c.start()
        sends.append(c)
        return c

    bufs = (all_tok, all_cot, all_meta)
    ring_copies = {}
    mate_copies = []
    plan = {(step, d): items for step, d, items in ring_plan(length)}

    def ring_send(step, d, item, src):
        dest = nxt if d == 0 else prv
        subs = (0, 2) if item == 0 else (1,)
        for b in subs:
            n = ((step - 1) * 2 + d) * 3 + b
            ring_copies[step, d, b] = remote(
                bufs[b].at[src], bufs[b].at[src], ring_s.at[n], ring_r.at[n], {"ep": dest}
            )

    def mate_send(item, src):
        for b in (0, 2) if item == 0 else (1,):
            n = len(mate_copies)
            mate_copies.append(
                remote(
                    bufs[b].at[src], bufs[b].at[src], mate_s.at[n], mate_r.at[n], {"ep": mate}
                )
            )

    for c in owns:
        c.wait()
    for pos in range(2):
        for d in range(2):
            items = plan.get((1, d), ())
            if pos < len(items):
                ring_send(1, d, items[pos], me)
    mate_send(0, me)
    mate_send(1, me)

    tp_order = [(mt + o) % tp for o in range(1, tp)]
    if rpt * tp > tok:
        sh_part[:, tok:, :] = jnp.zeros((3, rpt * tp - tok, sff), BF)
    for n in range(3):
        loads[n].wait()
        if n < 2:
            val = dot(all_tok[me], (sg, su)[n][...])
        else:
            val = dot_t(all_cot[me], sd[...])
        sh_part[n, :tok, :] = val.astype(BF)
    sh_copies = []
    for o in range(1, tp):
        peer = tp_order[o - 1]
        sh_copies.append(
            remote(
                sh_part.at[:, pl.ds(pl.multiple_of(peer * rpt, 16), rpt), :],
                sh_recv.at[o],
                shr_s.at[o],
                shr_r.at[o],
                {"tp": peer},
            )
        )

    def ring_arrivals(step):
        for pos in range(2):
            for d in range(2):
                items = plan.get((step, d), ())
                if pos >= len(items):
                    continue
                item = items[pos]
                away = length - step if d == 0 else step
                src = ((chip + away) % length) * CORES + core
                for b in (0, 2) if item == 0 else (1,):
                    ring_copies[step, d, b].wait_recv()
                if item in plan.get((step + 1, d), ()):
                    ring_send(step + 1, d, item, src)
                mate_send(item, src)

    if length > 1:
        ring_arrivals(1)

    for c in sh_copies:
        c.wait_recv()
    mine_t = pl.ds(pl.multiple_of(mt * rpt, 16), rpt)
    tot = [sh_part[n, mine_t, :].astype(F32) for n in range(3)]
    for o in range(1, tp):
        for n in range(3):
            tot[n] = tot[n] + sh_recv[o, n].astype(F32)
    a, b, c3, _ = hidden_terms(tot[0], tot[1], tot[2], None)
    sh_all[0, mine_t, :] = a
    sh_all[1, mine_t, :] = b
    sh_all[2, mine_t, :] = c3
    sha = []
    for o in range(1, tp):
        sha.append(
            remote(
                sh_all.at[:, mine_t, :],
                sh_all.at[:, mine_t, :],
                sha_s.at[o],
                sha_r.at[o],
                {"tp": tp_order[o - 1]},
            )
        )

    for step in range(2, length // 2 + 1):
        ring_arrivals(step)
    for c in mate_copies:
        c.wait_recv()

    row_id = lax.broadcasted_iota(jnp.int32, (rows, tok), 0)
    gate = jnp.zeros((rows, 1), F32)
    for j in range(ep):
        m = all_meta[j]
        code = m[0:2, :].astype(jnp.int32) + (j * cap - me * (ne * re))
        p0 = (row_id == code[0:1, :]).astype(F32)
        p1 = (row_id == code[1:2, :]).astype(F32)
        sel[:, j * tok : (j + 1) * tok] = (p0 + p1).astype(BF)
        gate = gate + jnp.sum(p0 * m[2:3, :] + p1 * m[3:4, :], axis=1, keepdims=True)
    te = rpp * tp
    for e in range(ne):
        gates[e, :re, :] = jnp.broadcast_to(gate[e * re : (e + 1) * re, :], (re, 128))
        if te > re:
            gates[e, re:, :] = jnp.zeros((te - re, 128), F32)
            part[e, :, re:, :] = jnp.zeros((3, te - re, ff), BF)
            exact[e, :, re:, :] = jnp.zeros((3, te - re, ff), F32)

    stok[...] = dot(sel[...], all_tok[...].reshape(ep * tok, dl)).astype(BF)
    scot[...] = dot(sel[...], all_cot[...].reshape(ep * tok, dl)).astype(BF)
    for n in range(3):
        loads[3 + n].wait()
    p_copies = [[] for _ in range(ne)]
    for e in range(ne):
        for n in range(3):
            r = slice(e * re, (e + 1) * re)
            val = dot_t(scot[r, :], ed[e]) if n == 2 else dot(stok[r, :], (eg, eu)[n][e])
            exact[e, n, :re, :] = val
            part[e, n, :re, :] = val.astype(BF)
            for o in range(1, tp):
                peer = tp_order[o - 1]
                k = (e * 3 + n) * tp + o
                p_copies[e].append(
                    remote(
                        part.at[e, n, pl.ds(pl.multiple_of(peer * rpp, 8), rpp), :],
                        recv.at[o, e, n],
                        pr_s.at[k],
                        pr_r.at[k],
                        {"tp": peer},
                    )
                )

    for c in sha:
        c.wait_recv()
    for n in range(3):
        back_t = sh_all[n, :tok, :].astype(F32).T.astype(BF)
        for j in range(ep):
            share_t[0, n, j] = back_t[j * swid : (j + 1) * swid, :]
    xts = []
    for o in range(1, ep):
        peer = (me + o) % ep
        xts.append(
            remote(
                share_t.at[0, :, peer],
                share_t.at[1, :, me],
                xt_s.at[o],
                xt_r.at[o],
                {"ep": peer},
            )
        )
    for n in range(3):
        share_t[1, n, me] = share_t[0, n, me]
    mine = pl.ds(pl.multiple_of(mt * rpp, 8), rpp)
    lane = lax.broadcasted_iota(jnp.int32, (rpp, 128), 1)
    pas = []
    for e in range(ne):
        for c in p_copies[e]:
            c.wait_recv()
        tot = [exact[e, n, mine, :] for n in range(3)]
        for o in range(1, tp):
            for n in range(3):
                tot[n] = tot[n] + recv[o, e, n].astype(F32)
        a, b, c3, dg = hidden_terms(tot[0], tot[1], tot[2], gates[e, mine, :][:, 0:1])
        hg[e, mine, :] = a
        hu[e, mine, :] = b
        hh[e, mine, :] = c3
        high = dg.astype(BF).astype(F32)
        dgs[e, mine, :] = jnp.where(
            lane == 0, high, jnp.where(lane == 1, dg - high, 0.0)
        ).astype(BF)
        group = []
        for k, buf in enumerate((hg, hu, dgs, hh)):
            for o in range(1, tp):
                n = (e * 4 + k) * tp + o
                group.append(
                    remote(
                        buf.at[e, mine, :],
                        buf.at[e, mine, :],
                        pa_s.at[n],
                        pa_r.at[n],
                        {"tp": tp_order[o - 1]},
                    )
                )
        pas.append(group)

    col = lax.broadcasted_iota(jnp.int32, (8, re), 1)
    block = jnp.zeros((8, re), jnp.int32)
    for j in range(1, ep):
        block = block + (col >= j * cap).astype(jnp.int32)
    target = block * cp + (col - block * cap)
    target = jnp.where(col < ep * cap, target, -1)
    pick = (
        (lax.broadcasted_iota(jnp.int32, (ep * cp, re), 0) == target[0:1, :])
        .astype(F32)
        .astype(BF)
    )
    bks = []
    for e in range(ne):
        for c in pas[e][: 3 * (tp - 1)]:
            c.wait_recv()
        slot = (dot_t(hg[e, :re, :], eg[e]) + dot_t(hu[e, :re, :], eu[e])).astype(BF)
        back_send[e, :, :, :dl] = dot(pick, slot).astype(BF).reshape(ep, cp, dl)
        back_send[e, :, :, dl:] = dot(pick, dgs[e, :re, :]).astype(BF).reshape(ep, cp, 128)
        for o in range(1, ep):
            peer = (me + o) % ep
            bks.append(
                remote(
                    back_send.at[e, peer],
                    back.at[e, me],
                    bk_s.at[e * ep + o],
                    bk_r.at[e * ep + o],
                    {"ep": peer},
                )
            )
        back[e, me] = back_send[e, me]

    shsum[...] = dot_t(sh_all[0, :tok, :], sg[...]) + dot_t(sh_all[1, :tok, :], su[...])
    for c in xts:
        c.wait_recv()
    flat = [
        jnp.concatenate([share_t[1, n, j] for j in range(ep)], axis=1) for n in range(3)
    ]
    tok_flat = all_tok[...].reshape(ep * tok, dl)
    osg[...] = dot(flat[0], tok_flat)
    osu[...] = dot(flat[1], tok_flat)
    osd[...] = dot(flat[2], all_cot[...].reshape(ep * tok, dl))

    width = ne * ep * cp
    home = all_meta[me].T.astype(jnp.int32)
    hcol = lax.broadcasted_iota(jnp.int32, (tok, width), 1)
    g0 = (hcol == home[:, 4:5]).astype(F32)
    g1 = (hcol == home[:, 5:6]).astype(F32)
    both = (g0 + g1).astype(BF)
    for c in bks:
        c.wait_recv()
    flat_back = back[...].reshape(width, dl + 128)
    gtok_out[...] = (dot(both, flat_back[:, :dl]) + shsum[...]).astype(BF)
    w0 = jnp.sum(dot(g0.astype(BF), flat_back[:, dl:]), axis=1, keepdims=True)
    w1 = jnp.sum(dot(g1.astype(BF), flat_back[:, dl:]), axis=1, keepdims=True)
    wl = lax.broadcasted_iota(jnp.int32, (tok, 128), 1)
    gw_out[...] = jnp.where(wl == 0, w0, w1).T[0:2, :]
    for group in pas:
        for c in group[3 * (tp - 1) :]:
            c.wait_recv()
    for c in sends:
        c.wait_send()


def body(
    tokens,
    routes,
    route_weights,
    cotangent,
    expert_gate,
    expert_up,
    expert_down,
    shared_gate,
    shared_up,
    shared_down,
):
    tok, top = routes.shape
    dl = tokens.shape[1]
    ne, _, ff = expert_gate.shape
    sff = shared_gate.shape[1]
    ep, tp = lax.axis_size("ep"), lax.axis_size("tp")
    cap = max(2, 5 * tok * top // (4 * ep * ne))
    re = up_to(ep * cap, 16)
    rows = ne * re
    rpp = up_to(-(-re // tp), 8)
    rpt = up_to(-(-tok // tp), 16)
    cp = up_to(cap, 8)
    swid = sff // ep
    length = ep // CORES
    total = rpp * tp
    dims = (ep, tp, tok, dl, ne, ff, sff, cap, re, rows, rpp, rpt, cp, swid)

    picked = routes.T.reshape(-1)
    earlier = jnp.arange(top * tok)[None, :] < jnp.arange(top * tok)[:, None]
    same = picked[:, None] == picked[None, :]
    ranked = jnp.sum((same & earlier).astype(jnp.int32), axis=1)
    code = (picked * re + ranked).reshape(top, tok)
    home = (((picked % ne) * ep + picked // ne) * cp + ranked).reshape(top, tok)
    gate = route_weights.astype(BF).astype(F32).T
    meta = jnp.concatenate(
        [code.astype(F32), gate, home.astype(F32), jnp.zeros((8 - 3 * top, tok), F32)], axis=0
    )

    vm = pl.BlockSpec(memory_space=pltpu.VMEM)
    hbm = pl.BlockSpec(memory_space=pl.ANY)
    dma = pltpu.SemaphoreType.DMA
    n_ring = max(1, (length // 2) * 6)
    scratch = [
        pltpu.VMEM((ep, tok, dl), BF),
        pltpu.VMEM((ep, tok, dl), BF),
        pltpu.VMEM((ep, 8, tok), F32),
        pltpu.VMEM(expert_gate.shape, BF),
        pltpu.VMEM(expert_up.shape, BF),
        pltpu.VMEM(expert_down.shape, BF),
        pltpu.VMEM(shared_gate.shape, BF),
        pltpu.VMEM(shared_up.shape, BF),
        pltpu.VMEM(shared_down.shape, BF),
        pltpu.VMEM((rows, ep * tok), BF),
        pltpu.VMEM((ne, total, 128), F32),
        pltpu.VMEM((3, rpt * tp, sff), BF),
        pltpu.VMEM((tp, 3, rpt, sff), BF),
        pltpu.VMEM((3, rpt * tp, sff), BF),
        pltpu.VMEM((2, 3, ep, swid, tok), BF),
        pltpu.VMEM((ne, 3, total, ff), BF),
        pltpu.VMEM((ne, 3, total, ff), F32),
        pltpu.VMEM((tp, ne, 3, rpp, ff), BF),
        pltpu.VMEM((ne, total, 128), BF),
        pltpu.VMEM((ne, ep, cp, dl + 128), BF),
        pltpu.VMEM((ne, ep, cp, dl + 128), BF),
        pltpu.VMEM((tok, dl), F32),
        dma((6,)),
        dma((3,)),
        dma((n_ring,)),
        dma((n_ring,)),
        dma((3 * length,)),
        dma((3 * length,)),
        dma((tp,)),
        dma((tp,)),
        dma((tp,)),
        dma((tp,)),
        dma((3 * ne * tp,)),
        dma((3 * ne * tp,)),
        dma((4 * ne * tp,)),
        dma((4 * ne * tp,)),
        dma((ep,)),
        dma((ep,)),
        dma((ne * ep,)),
        dma((ne * ep,)),
    ]
    sds = jax.ShapeDtypeStruct
    outs = pl.pallas_call(
        functools.partial(kernel, dims),
        out_shape=(
            sds((tok, dl), BF),
            sds((top, tok), F32),
            sds((swid, dl), F32),
            sds((swid, dl), F32),
            sds((swid, dl), F32),
            sds((rows, dl), BF),
            sds((rows, dl), BF),
            sds((ne, total, ff), BF),
            sds((ne, total, ff), BF),
            sds((ne, total, ff), BF),
        ),
        in_specs=[hbm] * 9,
        out_specs=tuple([vm] * 10),
        scratch_shapes=scratch,
        compiler_params=pltpu.CompilerParams(
            collective_id=0, has_side_effects=True, vmem_limit_bytes=60 * 1024 * 1024
        ),
    )(
        meta,
        tokens,
        cotangent,
        expert_gate,
        expert_up,
        expert_down,
        shared_gate,
        shared_up,
        shared_down,
    )
    gtok, gw, osg, osu, osd, stok, scot, hg, hu, hh = outs
    stok = stok.reshape(ne, re, dl)
    scot = scot.reshape(ne, re, dl)
    hg, hu, hh = (h[:, :re] for h in (hg, hu, hh))
    grad_gate = jnp.einsum("esd,esf->edf", stok, hg, preferred_element_type=F32)
    grad_up = jnp.einsum("esd,esf->edf", stok, hu, preferred_element_type=F32)
    grad_down = jnp.einsum("esf,esd->efd", hh, scot, preferred_element_type=F32)
    return gtok, gw.T, grad_gate, grad_up, grad_down, osg.T, osu.T, osd


def solution(mesh):
    return jax.shard_map(
        body,
        mesh=mesh,
        in_specs=(
            P("ep", "tp"),
            P("ep", None),
            P("ep", None),
            P("ep", "tp"),
            P("ep", "tp", None),
            P("ep", "tp", None),
            P("ep", None, "tp"),
            P("tp", None),
            P("tp", None),
            P(None, "tp"),
        ),
        out_specs=(
            P("ep", "tp"),
            P("ep", None),
            P("ep", "tp", None),
            P("ep", "tp", None),
            P("ep", None, "tp"),
            P("tp", "ep"),
            P("tp", "ep"),
            P("ep", "tp"),
        ),
        check_vma=False,
    )
```

profile of v0, /device:TPU:0, one launch (start us, length us, event | category | flops | bytes accessed | tf_op | source)
XLA Modules:
  0.0 103.7 jit_solution(17867800190848218114)
XLA Ops:
  0.6 0.1 pad.3.clone
  0.7 0.7 convert_bitcast_fusion
  1.4 0.9 convert_reduce_fusion
  2.3 0.7 fusion.3
  3.0 0.7 maximum_maximum_fusion.meta_in
  3.7 86.8 %shard_map.161 = (bf16[128,1024]{1,0:T(8,128)(2,1)}, f32[2,128]{1,0:T(2,128)}, f32[64,1024]{1,0:T(8,128)}, f32[64,1024]{1,0:T(8,128)}, f32[64,1024]{1,0:T(8,128)...) custom-call(f32[8,128]{1,0:T(8,128)} %maximum_maximum_fusion.meta_in, ...), custom_call_target="tpu_custom_call" | custom-call | tf_op jit(solution)/shard_map/pallas_call | solution.py:498
  90.5 0.0 copy-start
  90.5 0.0 copy-start.3
  90.5 0.0 copy-start.1
  90.5 0.0 copy-start.2
  90.5 4.1 %fusion.6 = f32[2,1024,512]{2,1,0:T(8,128)} fusion(bf16[2,160,1024]{2,1,0:T(8,128)(2,1)} %bitcast.35, bf16[2,160,512]{2,1,0:T(8,128)(2,1)} %get-tuple-element.22), kind=kOutput, calls=%fused_computation.19 | convolution fusion | flops 335544320 | bytes 5177344 | tf_op jit(solution)/shard_map/esd,esf->edf/dot_general | solution.py:534
  94.7 0.0 copy-done
  94.7 0.0 copy-done.3
  94.7 0.0 copy-start.7
  94.7 0.0 copy-start.8
  94.7 0.0 copy-start.6
  94.7 2.8 %fusion.5 = f32[2,1024,512]{2,1,0:T(8,128)} fusion(bf16[2,160,1024]{2,1,0:T(8,128)(2,1)S(1)} %bitcast.36, bf16[2,160,512]{2,1,0:T(8,128)(2,1)S(1)} %copy-done.3), kind=kOutput, calls=%fused_computation.18 | convolution fusion | flops 335544320 | bytes 5177344 | tf_op jit(solution)/shard_map/esd,esf->edf/dot_general | solution.py:533
  97.5 0.0 copy-done.1
  97.5 0.0 copy-done.2
  97.5 0.0 copy-start.5
  97.5 0.0 copy-start.4
  97.5 2.8 %fusion.7 = f32[2,512,1024]{2,1,0:T(8,128)} fusion(bf16[2,160,512]{2,1,0:T(8,128)(2,1)S(1)} %copy-done.2, bf16[2,160,1024]{2,1,0:T(8,128)(2,1)S(1)} %bitcast.37), kind=kOutput, calls=%fused_computation.20 | convolution fusion | flops 335544320 | bytes 5177344 | tf_op jit(solution)/shard_map/esf,esd->efd/dot_general | solution.py:535
  100.3 0.0 copy-done.7
  100.3 0.7 copy.23
  101.0 0.0 copy-done.8
  101.0 0.6 copy.24
  101.6 0.0 copy-done.6
  101.6 0.7 copy.25
  102.3 0.0 copy-done.5
  102.3 0.7 copy.26
  103.0 0.0 copy-done.4
  103.0 0.7 copy.27
  (1 shorter events, 0.0 us)
Async XLA Ops:
  90.5 4.2 %copy-start = (bf16[320,1024]{1,0:T(8,128)(2,1)S(1)}, bf16[320,1024]{1,0:T(8,128)(2,1)}, u32[]{:S(2)}) copy-start(bf16[320,1024]{1,0:T(8,128)(2,1)} %get-tuple-element.20) | copy-start | bytes 1966084
  90.5 4.2 %copy-start.3 = (bf16[2,160,512]{2,1,0:T(8,128)(2,1)S(1)}, bf16[2,160,512]{2,1,0:T(8,128)(2,1)}, u32[]{:S(2)}) copy-start(bf16[2,160,512]{2,1,0:T(8,128)(2,1)} %get-tuple-element.21) | copy-start | bytes 983044
  90.5 7.0 %copy-start.1 = (bf16[320,1024]{1,0:T(8,128)(2,1)S(1)}, bf16[320,1024]{1,0:T(8,128)(2,1)}, u32[]{:S(2)}) copy-start(bf16[320,1024]{1,0:T(8,128)(2,1)} %get-tuple-element.24) | copy-start | bytes 1966084
  90.5 7.0 %copy-start.2 = (bf16[2,160,512]{2,1,0:T(8,128)(2,1)S(1)}, bf16[2,160,512]{2,1,0:T(8,128)(2,1)}, u32[]{:S(2)}) copy-start(bf16[2,160,512]{2,1,0:T(8,128)(2,1)} %get-tuple-element.23) | copy-start | bytes 983044
  94.7 5.7 %copy-start.7 = (bf16[128,1024]{1,0:T(8,128)(2,1)S(1)}, bf16[128,1024]{1,0:T(8,128)(2,1)}, u32[]{:S(2)}) copy-start(bf16[128,1024]{1,0:T(8,128)(2,1)} %get-tuple-element.38) | copy-start | bytes 786436
  94.7 6.4 %copy-start.8 = (f32[2,128]{1,0:T(2,128)S(1)}, f32[2,128]{1,0:T(2,128)}, u32[]{:S(2)}) copy-start(f32[2,128]{1,0:T(2,128)} %get-tuple-element.19) | copy-start | bytes 3076
  94.7 6.9 %copy-start.6 = (f32[64,1024]{1,0:T(8,128)S(1)}, f32[64,1024]{1,0:T(8,128)}, u32[]{:S(2)}) copy-start(f32[64,1024]{1,0:T(8,128)} %get-tuple-element.25) | copy-start | bytes 786436
  97.5 4.8 %copy-start.5 = (f32[64,1024]{1,0:T(8,128)S(1)}, f32[64,1024]{1,0:T(8,128)}, u32[]{:S(2)}) copy-start(f32[64,1024]{1,0:T(8,128)} %get-tuple-element.26) | copy-start | bytes 786436
  97.5 5.5 %copy-start.4 = (f32[64,1024]{1,0:T(8,128)S(1)}, f32[64,1024]{1,0:T(8,128)}, u32[]{:S(2)}) copy-start(f32[64,1024]{1,0:T(8,128)} %get-tuple-element.45) | copy-start | bytes 786436
where the time goes:
time: 105 us; the launch traced here: 104 us
  Pallas kernels  86.8 us (83%)
  matrix products  9.76 us (9%)
  local copies, waits for them, and re-layouts  3.49 us (3%)
  other arithmetic  2.97 us (3%)
    pallas_call x1, Pallas kernels, body(): pl.pallas_call(functools.partial(kernel, dims), out_shape=(sds((tok, dl),...  86.8 us
    dot_general x1, matrix products, body(): grad_up = jnp.einsum('esd,esf->edf', stok, hu, preferred_element_type=F32)  4.14 us
    unnamed x23, local copies, waits for them, and re-layouts  3.41 us
    dot_general x1, matrix products, body(): grad_gate = jnp.einsum('esd,esf->edf', stok, hg, preferred_element_type=F32)  2.84 us
    dot_general x1, matrix products, body(): grad_down = jnp.einsum('esf,esd->efd', hh, scot, preferred_element_type=F32)  2.78 us

commit v1 on v0

--- a/solution.py
+++ b/solution.py
@@ -48,7 +48,7 @@
     return plan
 
 
-def kernel(
+def rows_kernel(
     dims,
     meta_in,
     tok_in,
@@ -409,7 +409,7 @@
         c.wait_send()
 
 
-def body(
+def rows_body(
     tokens,
     routes,
     route_weights,
@@ -496,7 +496,7 @@
     ]
     sds = jax.ShapeDtypeStruct
     outs = pl.pallas_call(
-        functools.partial(kernel, dims),
+        functools.partial(rows_kernel, dims),
         out_shape=(
             sds((tok, dl), BF),
             sds((top, tok), F32),
@@ -536,6 +536,616 @@
     return gtok, gw.T, grad_gate, grad_up, grad_down, osg.T, osu.T, osd
 
 
+def line_order(chip, length):
+    high = (2 * chip) // length
+    far = 1 - 2 * high
+    edge = chip * (1 - high) + (length - 1 - chip) * high
+    order = [(chip, None, None)]
+    for p in range(1, length):
+        two_sided = (2 * edge - p + 2 * length) // (2 * length)
+        dist = two_sided * ((p + 1) // 2) + (1 - two_sided) * (p - edge)
+        toward = far * (1 - 2 * two_sided * (p % 2))
+        order.append((chip + toward * dist, chip - toward, two_sided))
+    return order
+
+
+def line_kernel(
+    dims,
+    meta_in,
+    tok_in,
+    cot_in,
+    eg_in,
+    eu_in,
+    ed_in,
+    sg_in,
+    su_in,
+    sd_in,
+    gtok_out,
+    gw_out,
+    osg,
+    osu,
+    osd,
+    stok,
+    scot,
+    hg,
+    hu,
+    hh,
+    all_tok,
+    all_cot,
+    all_meta,
+    eg,
+    eu,
+    ed,
+    sg,
+    su,
+    sd,
+    gates,
+    sh_part,
+    sh_exact,
+    sh_recv,
+    sh_all,
+    share_t,
+    part,
+    exact,
+    recv,
+    hs,
+    dgp,
+    dgs,
+    dgb,
+    back_send,
+    back,
+    shsum,
+    load_sem,
+    own_sem,
+    own_s,
+    line_s,
+    line_r,
+    mate_s,
+    mate_r,
+    shr_s,
+    shr_r,
+    sha_s,
+    sha_r,
+    pr_s,
+    pr_r,
+    pa_s,
+    pa_r,
+    xt_s,
+    xt_r,
+    bk_s,
+    bk_r,
+):
+    ep, tp, tok, dl, ne, ff, sff, cap, rows, width, swidth, swid = dims
+    me = lax.axis_index("ep")
+    mt = lax.axis_index("tp")
+    length = ep // CORES
+    chip = me // CORES
+    core = me % CORES
+    mate = chip * CORES + (1 - core)
+    pair = CORES * cap
+    group = ne * pair
+    home = ne * cap
+    order = line_order(chip, length)
+    bufs = (all_tok, all_meta, all_cot)
+
+    owns = []
+    for n, (src, dst) in enumerate(((tok_in, all_tok), (meta_in, all_meta), (cot_in, all_cot))):
+        c = pltpu.make_async_copy(src, dst.at[chip, core], own_sem.at[n])
+        c.start()
+        owns.append(c)
+    loads = []
+    for n, (src, dst) in enumerate(
+        ((sg_in, sg), (su_in, su), (sd_in, sd), (eg_in, eg), (eu_in, eu), (ed_in, ed))
+    ):
+        c = pltpu.make_async_copy(src, dst, load_sem.at[n])
+        c.start()
+        loads.append(c)
+
+    barrier = pltpu.get_barrier_semaphore()
+    for o in range(1, ep):
+        pl.semaphore_signal(barrier, inc=1, device_id={"ep": (me + o) % ep})
+    for o in range(1, tp):
+        pl.semaphore_signal(barrier, inc=1, device_id={"tp": (mt + o) % tp})
+    pl.semaphore_wait(barrier, ep + tp - 2)
+
+    sends = []
+
+    def copy_of(src, dst, ssem, rsem, dev):
+        return pltpu.make_async_remote_copy(
+            src_ref=src, dst_ref=dst, send_sem=ssem, recv_sem=rsem, device_id=dev
+        )
+
+    def remote(src, dst, ssem, rsem, dev):
+        c = copy_of(src, dst, ssem, rsem, dev)
+        c.start()
+        sends.append((None, c))
+        return c
+
+    def along_line(b, src, ssem, there):
+        block = bufs[b].at[src, core]
+        dest = ((there + length) % length) * CORES + core
+        return copy_of(block, block, ssem, line_r.at[b * length + src], {"ep": dest})
+
+    def to_mate(b, p):
+        block = bufs[b].at[order[p][0], core]
+        n = b * length + p
+        return copy_of(block, block, mate_s.at[n], mate_r.at[n], {"ep": mate})
+
+    for b in range(3):
+        owns[b].wait()
+        for d, there in enumerate((chip + 1, chip - 1)):
+            c = along_line(b, chip, own_s.at[2 * b + d], there)
+            inside = chip < length - 1 if d == 0 else chip > 0
+            pl.when(inside)(c.start)
+            sends.append((inside, c))
+        c = to_mate(b, 0)
+        c.start()
+        sends.append((None, c))
+
+    relays = {}
+    mates = {}
+    for p in range(1, length):
+        src, there, _ = order[p]
+        for b in range(3):
+            relays[b, p] = along_line(b, src, line_s.at[b * length + p], there)
+            mates[b, p] = to_mate(b, p)
+            sends.append(((there >= 0) & (there < length), relays[b, p]))
+            sends.append((None, mates[b, p]))
+
+    def arrivals(p, which, cond=None):
+        def run():
+            _, there, _ = order[p]
+            for b in which:
+                relays[b, p].wait_recv()
+                pl.when((there >= 0) & (there < length))(relays[b, p].start)
+                mates[b, p].start()
+
+        if cond is None:
+            run()
+        else:
+            pl.when(cond)(run)
+
+    def mate_wait(p, which):
+        for b in which:
+            to_mate(b, p).wait_recv()
+
+    peers = [(mt + o) % tp for o in range(1, tp)]
+
+    own_tok = all_tok[chip, core]
+    own_cot = all_cot[chip, core]
+    for n in range(3):
+        loads[n].wait()
+        val = dot(own_tok, (sg, su)[n][...]) if n < 2 else dot_t(own_cot, sd[...])
+        for q in range(tp):
+            piece = val[:, q * swidth : (q + 1) * swidth]
+            sh_exact[q, n] = piece
+            sh_part[q, n] = piece.astype(BF)
+    sh_copies = []
+    for o in range(1, tp):
+        sh_copies.append(
+            remote(
+                sh_part.at[peers[o - 1]],
+                sh_recv.at[o],
+                shr_s.at[o],
+                shr_r.at[o],
+                {"tp": peers[o - 1]},
+            )
+        )
+
+    row_id = lax.broadcasted_iota(jnp.int32, (ne * rows, tok), 0)
+    sels = {}
+    pr_copies = {}
+
+    def selection(p):
+        src = order[p][0]
+        halves = []
+        gate = jnp.zeros((ne * rows, 1), F32)
+        for jj in range(CORES):
+            m = all_meta[src, jj]
+            code = m[0:2, :].astype(jnp.int32) + (jj * cap - me * (ne * rows))
+            p0 = (row_id == code[0:1, :]).astype(F32)
+            p1 = (row_id == code[1:2, :]).astype(F32)
+            halves.append((p0 + p1).astype(BF))
+            gate = gate + jnp.sum(p0 * m[2:3, :] + p1 * m[3:4, :], axis=1, keepdims=True)
+        sels[p] = jnp.concatenate(halves, axis=1)
+        gate = jnp.concatenate([gate[e * rows : e * rows + pair] for e in range(ne)], axis=0)
+        gates[p] = jnp.broadcast_to(gate, (group, 128))
+
+    def products(p, which):
+        src = order[p][0]
+        buf, out = (all_cot, scot) if which == (2,) else (all_tok, stok)
+        picked = dot(sels[p], buf[src].reshape(CORES * tok, dl)).astype(BF)
+        for e in range(ne):
+            out[e, p * rows : (p + 1) * rows, :] = picked[e * rows : (e + 1) * rows]
+        for n in which:
+            vals = []
+            for e in range(ne):
+                x = picked[e * rows : (e + 1) * rows]
+                val = dot_t(x, ed[e]) if n == 2 else dot(x, (eg, eu)[n][e])
+                vals.append(val[:pair])
+            val = jnp.concatenate(vals, axis=0)
+            for q in range(tp):
+                piece = val[:, q * width : (q + 1) * width]
+                exact[p, q, n] = piece
+                part[p, q, n] = piece.astype(BF)
+        half = 1 if which == (2,) else 0
+        span = pl.ds(which[0], len(which))
+        for o in range(1, tp):
+            k = (p * 2 + half) * tp + o
+            pr_copies[p, half, o] = remote(
+                part.at[p, peers[o - 1], span],
+                recv.at[p, o, span],
+                pr_s.at[k],
+                pr_r.at[k],
+                {"tp": peers[o - 1]},
+            )
+
+    def products_all(p):
+        selection(p)
+        products(p, (0, 1))
+        products(p, (2,))
+
+    pa_copies = {}
+
+    def hidden(p):
+        for half in range(2):
+            for o in range(1, tp):
+                pr_copies[p, half, o].wait_recv()
+        tot = [exact[p, mt, n] for n in range(3)]
+        for o in range(1, tp):
+            for n in range(3):
+                tot[n] = tot[n] + recv[p, o, n].astype(F32)
+        gate = gates[p][:, 0:1]
+        logistic = jax.nn.sigmoid(tot[0])
+        silu = tot[0] * logistic
+        product = silu * tot[1]
+        grad_act = gate * tot[2]
+        hs[p, mt, 0] = (
+            grad_act * tot[1] * logistic * (1.0 + tot[0] * (1.0 - logistic))
+        ).astype(BF)
+        hs[p, mt, 1] = (grad_act * silu).astype(BF)
+        hs[p, mt, 2] = (gate * product).astype(BF)
+        terms = tot[2] * product
+        fill = jnp.zeros((128 - group, width), F32)
+        cols = jnp.concatenate([terms, fill], axis=0).T
+        dgp[p, mt] = jnp.broadcast_to(jnp.sum(cols, axis=0, keepdims=True), (8, 128))
+        for piece in range(3):
+            for o in range(1, tp):
+                k = (p * 3 + piece) * tp + o
+                if piece < 2:
+                    block = hs.at[p, mt, pl.ds(2 * piece, 2 - piece)]
+                else:
+                    block = dgp.at[p, mt]
+                pa_copies[p, piece, o] = remote(
+                    block, block, pa_s.at[k], pa_r.at[k], {"tp": peers[o - 1]}
+                )
+
+    def pick_rows():
+        at = lax.broadcasted_iota(jnp.int32, (group, group), 0)
+        col = lax.broadcasted_iota(jnp.int32, (group, group), 1)
+        wanted = at * 0
+        for jj in range(CORES):
+            for e in range(ne):
+                low = jj * home + e * cap
+                inside = (at >= low) & (at < low + cap)
+                wanted = jnp.where(inside, at - low + e * pair + jj * cap, wanted)
+        return (col == wanted).astype(F32).astype(BF)
+
+    pick = pick_rows()
+    bk_copies = []
+
+    def spread(p, n, out):
+        full = jnp.concatenate([hs[p, q, n] for q in range(tp)], axis=1).astype(F32)
+        fill = jnp.zeros((rows - pair, ff), F32)
+        blocks = []
+        for e in range(ne):
+            block = full[e * pair : (e + 1) * pair]
+            if rows > pair:
+                block = jnp.concatenate([block, fill], axis=0)
+            block = block.astype(BF)
+            out[e, p * rows : (p + 1) * rows, :] = block
+            blocks.append(block)
+        return blocks
+
+    def slots(p):
+        src = order[p][0]
+        for o in range(1, tp):
+            pa_copies[p, 0, o].wait_recv()
+        a = spread(p, 0, hg)
+        b = spread(p, 1, hu)
+        vals = [(dot_t(a[e], eg[e]) + dot_t(b[e], eu[e]))[:pair] for e in range(ne)]
+        slot = jnp.concatenate(vals, axis=0).astype(BF)
+        moved = dot(pick, slot)
+        for jj in range(CORES):
+            back_send[p, jj] = moved[jj * home : (jj + 1) * home].astype(BF)
+        for o in range(1, tp):
+            pa_copies[p, 2, o].wait_recv()
+        total = dgp[p, 0]
+        for q in range(1, tp):
+            total = total + dgp[p, q]
+        dgs[p] = total
+        if p == 0:
+            back[me] = back_send[0, core]
+            dgb[me] = total
+            targets = [(1 - core, mate)]
+        else:
+            targets = [(jj, src * CORES + jj) for jj in range(CORES)]
+        for n, (jj, dest) in enumerate(targets):
+            k = p * CORES + n
+            bk_copies.append(
+                remote(back_send.at[p, jj], back.at[me], bk_s.at[2 * k], bk_r.at[me], {"ep": dest})
+            )
+            bk_copies.append(
+                remote(dgs.at[p], dgb.at[me], bk_s.at[2 * k + 1], bk_r.at[ep + me], {"ep": dest})
+            )
+
+    def shared_hidden():
+        for c in sh_copies:
+            c.wait_recv()
+        tot = [sh_exact[mt, n] for n in range(3)]
+        for o in range(1, tp):
+            for n in range(3):
+                tot[n] = tot[n] + sh_recv[o, n].astype(F32)
+        a, b, c3, _ = hidden_terms(tot[0], tot[1], tot[2], None)
+        sh_all[mt, 0] = a
+        sh_all[mt, 1] = b
+        sh_all[mt, 2] = c3
+        return [
+            remote(sh_all.at[mt], sh_all.at[mt], sha_s.at[o], sha_r.at[o], {"tp": peers[o - 1]})
+            for o in range(1, tp)
+        ]
+
+    def shared_full(n):
+        return jnp.concatenate([sh_all[q, n] for q in range(tp)], axis=1)
+
+    def shared_shares():
+        for n in range(3):
+            back_t = shared_full(n).astype(F32).T.astype(BF)
+            for j in range(ep):
+                share_t[0, n, j] = back_t[j * swid : (j + 1) * swid, :]
+        copies = []
+        for o in range(1, ep):
+            peer = (me + o) % ep
+            copies.append(
+                remote(
+                    share_t.at[0, :, peer],
+                    share_t.at[1, :, me],
+                    xt_s.at[o],
+                    xt_r.at[o],
+                    {"ep": peer},
+                )
+            )
+        for n in range(3):
+            share_t[1, n, me] = share_t[0, n, me]
+        return copies
+
+    mate_wait(0, (0, 1))
+    for n in range(3):
+        loads[3 + n].wait()
+    mate_wait(0, (2,))
+    products_all(0)
+    sha = shared_hidden()
+    hidden(0)
+    last = length - 1
+    for p in range(1, length):
+        two_sided = order[p][2]
+        split = p == last and p > 1
+        first = (0, 1) if split else (0, 1, 2)
+        if p % 2 == 1 or p == 1:
+            arrivals(p, first)
+            if p + 1 < length:
+                arrivals(p + 1, (0, 1, 2), order[p + 1][2] > 0)
+        else:
+            arrivals(p, first, two_sided < 1)
+        mate_wait(p, (0, 1))
+        selection(p)
+        products(p, (0, 1))
+        if split:
+            slots(p - 1)
+            for c in sha:
+                c.wait_recv()
+            xts = shared_shares()
+            arrivals(p, (2,))
+        mate_wait(p, (2,))
+        products(p, (2,))
+        if not split:
+            slots(p - 1)
+        hidden(p)
+    if last <= 1:
+        for c in sha:
+            c.wait_recv()
+        xts = shared_shares()
+    shsum[...] = dot_t(shared_full(0), sg[...]) + dot_t(shared_full(1), su[...])
+    slots(last)
+
+    for c in xts:
+        c.wait_recv()
+    flat = [
+        jnp.concatenate([share_t[1, n, j] for j in range(ep)], axis=1) for n in range(3)
+    ]
+    tok_flat = all_tok[...].reshape(ep * tok, dl)
+    osg[...] = dot(flat[0], tok_flat)
+    osu[...] = dot(flat[1], tok_flat)
+    osd[...] = dot(flat[2], all_cot[...].reshape(ep * tok, dl))
+
+    for p in range(length):
+        for o in range(1, tp):
+            pa_copies[p, 1, o].wait_recv()
+        spread(p, 2, hh)
+
+    own_meta = all_meta[chip, core]
+    where_home = own_meta.T.astype(jnp.int32)
+    hcol = lax.broadcasted_iota(jnp.int32, (tok, home), 1)
+    lane_at = lax.broadcasted_iota(jnp.int32, (ep * 128, tok), 0)
+    lanes = own_meta[6:8, :].astype(jnp.int32) + core * cap
+    spots = [(lane_at == lanes[k : k + 1, :]).astype(F32).astype(BF) for k in range(2)]
+    spots = jnp.concatenate(spots, axis=1)
+    for o in range(1, ep):
+        peer = (me + o) % ep
+        copy_of(back.at[peer], back.at[peer], bk_s.at[0], bk_r.at[peer], {"ep": peer}).wait_recv()
+        copy_of(dgb.at[peer], dgb.at[peer], bk_s.at[0], bk_r.at[ep + peer], {"ep": peer}).wait_recv()
+    grad = shsum[...]
+    for j in range(ep):
+        g0 = (hcol == where_home[:, 4:5] - j * home).astype(F32)
+        g1 = (hcol == where_home[:, 5:6] - j * home).astype(F32)
+        grad = grad + dot((g0 + g1).astype(BF), back[j])
+    gtok_out[...] = grad.astype(BF)
+    dg = jnp.concatenate([dgb[j] for j in range(ep)], axis=1)
+    high = dg.astype(BF)
+    low = (dg - high.astype(F32)).astype(BF)
+    gw = dot(high, spots) + dot(low, spots)
+    gw_out[...] = jnp.concatenate([gw[0:1, :tok], gw[0:1, tok:]], axis=0)
+    for cond, c in sends:
+        if cond is None:
+            c.wait_send()
+        else:
+            pl.when(cond)(c.wait_send)
+
+
+def line_body(
+    tokens,
+    routes,
+    route_weights,
+    cotangent,
+    expert_gate,
+    expert_up,
+    expert_down,
+    shared_gate,
+    shared_up,
+    shared_down,
+):
+    tok, top = routes.shape
+    dl = tokens.shape[1]
+    ne, _, ff = expert_gate.shape
+    sff = shared_gate.shape[1]
+    ep, tp = lax.axis_size("ep"), lax.axis_size("tp")
+    cap = max(2, 5 * tok * top // (4 * ep * ne))
+    length = ep // CORES
+    pair = CORES * cap
+    rows = up_to(pair, 16)
+    group = ne * pair
+    home = ne * cap
+    width, swidth, swid = ff // tp, sff // tp, sff // ep
+    dims = (ep, tp, tok, dl, ne, ff, sff, cap, rows, width, swidth, swid)
+
+    picked = routes.T.reshape(-1)
+    earlier = jnp.arange(top * tok)[None, :] < jnp.arange(top * tok)[:, None]
+    same = picked[:, None] == picked[None, :]
+    ranked = jnp.sum((same & earlier).astype(jnp.int32), axis=1)
+    code = (picked * rows + ranked).reshape(top, tok)
+    place = ((picked // ne) * home + (picked % ne) * cap + ranked).reshape(top, tok)
+    lane = ((picked // ne) * 128 + (picked % ne) * pair + ranked).reshape(top, tok)
+    gate = route_weights.astype(BF).astype(F32).T
+    meta = jnp.concatenate(
+        [code.astype(F32), gate, place.astype(F32), lane.astype(F32)], axis=0
+    )
+
+    vm = pl.BlockSpec(memory_space=pltpu.VMEM)
+    hbm = pl.BlockSpec(memory_space=pl.ANY)
+    dma = pltpu.SemaphoreType.DMA
+    scratch = [
+        pltpu.VMEM((length, CORES, tok, dl), BF),
+        pltpu.VMEM((length, CORES, tok, dl), BF),
+        pltpu.VMEM((length, CORES, 8, tok), F32),
+        pltpu.VMEM(expert_gate.shape, BF),
+        pltpu.VMEM(expert_up.shape, BF),
+        pltpu.VMEM(expert_down.shape, BF),
+        pltpu.VMEM(shared_gate.shape, BF),
+        pltpu.VMEM(shared_up.shape, BF),
+        pltpu.VMEM(shared_down.shape, BF),
+        pltpu.VMEM((length, group, 128), F32),
+        pltpu.VMEM((tp, 3, tok, swidth), BF),
+        pltpu.VMEM((tp, 3, tok, swidth), F32),
+        pltpu.VMEM((tp, 3, tok, swidth), BF),
+        pltpu.VMEM((tp, 3, tok, swidth), BF),
+        pltpu.VMEM((2, 3, ep, swid, tok), BF),
+        pltpu.VMEM((length, tp, 3, group, width), BF),
+        pltpu.VMEM((length, tp, 3, group, width), F32),
+        pltpu.VMEM((length, tp, 3, group, width), BF),
+        pltpu.VMEM((length, tp, 3, group, width), BF),
+        pltpu.VMEM((length, tp, 8, 128), F32),
+        pltpu.VMEM((length, 8, 128), F32),
+        pltpu.VMEM((ep, 8, 128), F32),
+        pltpu.VMEM((length, CORES, home, dl), BF),
+        pltpu.VMEM((ep, home, dl), BF),
+        pltpu.VMEM((tok, dl), F32),
+        dma((6,)),
+        dma((3,)),
+        dma((6,)),
+        dma((3 * length,)),
+        dma((3 * length,)),
+        dma((3 * length,)),
+        dma((3 * length,)),
+        dma((tp,)),
+        dma((tp,)),
+        dma((tp,)),
+        dma((tp,)),
+        dma((2 * length * tp,)),
+        dma((2 * length * tp,)),
+        dma((3 * length * tp,)),
+        dma((3 * length * tp,)),
+        dma((ep,)),
+        dma((ep,)),
+        dma((2 * CORES * length,)),
+        dma((2 * ep,)),
+    ]
+    sds = jax.ShapeDtypeStruct
+    outs = pl.pallas_call(
+        functools.partial(line_kernel, dims),
+        out_shape=(
+            sds((tok, dl), BF),
+            sds((top, tok), F32),
+            sds((swid, dl), F32),
+            sds((swid, dl), F32),
+            sds((swid, dl), F32),
+            sds((ne, length * rows, dl), BF),
+            sds((ne, length * rows, dl), BF),
+            sds((ne, length * rows, ff), BF),
+            sds((ne, length * rows, ff), BF),
+            sds((ne, length * rows, ff), BF),
+        ),
+        in_specs=[hbm] * 9,
+        out_specs=tuple([vm] * 10),
+        scratch_shapes=scratch,
+        compiler_params=pltpu.CompilerParams(
+            collective_id=0, has_side_effects=True, vmem_limit_bytes=60 * 1024 * 1024
+        ),
+    )(
+        meta,
+        tokens,
+        cotangent,
+        expert_gate,
+        expert_up,
+        expert_down,
+        shared_gate,
+        shared_up,
+        shared_down,
+    )
+    gtok, gw, osg, osu, osd, stok, scot, hg, hu, hh = outs
+    grad_gate = jnp.einsum("esd,esf->edf", stok, hg, preferred_element_type=F32)
+    grad_up = jnp.einsum("esd,esf->edf", stok, hu, preferred_element_type=F32)
+    grad_down = jnp.einsum("esf,esd->efd", hh, scot, preferred_element_type=F32)
+    return gtok, gw.T, grad_gate, grad_up, grad_down, osg.T, osu.T, osd
+
+
+def body(tokens, routes, *rest):
+    tok, top = routes.shape
+    ne, _, ff = rest[2].shape
+    sff = rest[5].shape[1]
+    ep, tp = lax.axis_size("ep"), lax.axis_size("tp")
+    cap = max(2, 5 * tok * top // (4 * ep * ne))
+    lines = (
+        ff == tp * 128
+        and sff == tp * 128
+        and ep % CORES == 0
+        and (CORES * cap) % 8 == 0
+        and (ne * cap) % 8 == 0
+        and (ne * CORES * cap) % 16 == 0
+        and ne * CORES * cap <= 128
+    )
+    return (line_body if lines else rows_body)(tokens, routes, *rest)
+
+
 def solution(mesh):
     return jax.shard_map(
         body,

time: 105 us -> 91.3 us (0.87)
  Pallas kernels: 86.8 us -> 73.2 us
    pallas_call x1, Pallas kernels: 86.8 us -> 73.2 us  [line_body(): pl.pallas_call(functools.partial(line_kernel, dims), out_shape=(sds((tok,...]
where the time goes in v1:
time: 91.3 us; the launch traced here: 90.7 us
  Pallas kernels  73.2 us (80%)
  matrix products  9.84 us (11%)
  other arithmetic  3.61 us (4%)
  local copies, waits for them, and re-layouts  3.41 us (4%)
    pallas_call x1, Pallas kernels, line_body(): pl.pallas_call(functools.partial(line_kernel, dims), out_shape=(sds((tok,...  73.2 us
    dot_general x1, matrix products, line_body(): grad_gate = jnp.einsum('esd,esf->edf', stok, hg, preferred_element_type=F32)  4.22 us
    unnamed x23, local copies, waits for them, and re-layouts  3.41 us
    dot_general x1, matrix products, line_body(): grad_up = jnp.einsum('esd,esf->edf', stok, hu, preferred_element_type=F32)  2.83 us
    dot_general x1, matrix products, line_body(): grad_down = jnp.einsum('esf,esd->efd', hh, scot, preferred_element_type=F32)  2.78 us

profile of v1, /device:TPU:0, one launch (start us, length us, event | category | flops | bytes accessed | tf_op | source)
XLA Modules:
  0.0 90.7 jit_solution(17479423944459339480)
XLA Ops:
  0.6 0.9 %convert_reduce_fusion = s32[256]{0:T(256)S(1)} fusion(s32[256]{0:T(256)} %bitcast.53), kind=kLoop, calls=%fused_computation | loop fusion | flops 327424 | bytes 2048 | tf_op jit(solution)/shard_map/reduce_sum | solution.py:1034
  1.6 0.7 convert_bitcast_fusion
  2.3 0.7 fusion.2
  2.9 0.7 fusion.3
  3.6 0.6 pad_maximum_fusion.meta_in
  4.2 73.2 %shard_map.161 = (bf16[128,1024]{1,0:T(8,128)(2,1)}, f32[2,128]{1,0:T(2,128)}, f32[64,1024]{1,0:T(8,128)}, f32[64,1024]{1,0:T(8,128)}, f32[64,1024]{1,0:T(8,128)...) custom-call(f32[8,128]{1,0:T(8,128)} %pad_maximum_fusion.meta_in, ...), custom_call_target="tpu_custom_call" | custom-call | tf_op jit(solution)/shard_map/pallas_call | solution.py:1093
  77.4 0.0 copy-start
  77.4 0.0 copy-start.3
  77.4 0.0 copy-start.1
  77.4 0.0 copy-start.2
  77.4 4.2 %fusion.4 = f32[2,1024,512]{2,1,0:T(8,128)} fusion(bf16[2,192,1024]{2,1,0:T(8,128)(2,1)} %get-tuple-element.20, bf16[2,192,512]{2,1,0:T(8,128)(2,1)} %get-tuple-element.21), kind=kOutput, calls=%fused_computation.20 | convolution fusion | flops 402653184 | bytes 5373952 | tf_op jit(solution)/shard_map/esd,esf->edf/dot_general | solution.py:1125
  81.7 0.0 copy-done
  81.7 0.0 copy-done.3
  81.7 0.0 copy-start.7
  81.7 2.8 %fusion.5 = f32[2,1024,512]{2,1,0:T(8,128)} fusion(bf16[2,192,1024]{2,1,0:T(8,128)(2,1)S(1)} %copy-done, bf16[2,192,512]{2,1,0:T(8,128)(2,1)S(1)} %copy-done.3), kind=kOutput, calls=%fused_computation.21 | convolution fusion | flops 402653184 | bytes 5373952 | tf_op jit(solution)/shard_map/esd,esf->edf/dot_general | solution.py:1126
  84.5 0.0 copy-done.1
  84.5 0.0 copy-done.2
  84.5 0.0 copy-start.8
  84.5 0.0 copy-start.6
  84.5 0.0 copy-start.5
  84.5 0.0 copy-start.4
  84.5 2.8 %fusion.6 = f32[2,512,1024]{2,1,0:T(8,128)} fusion(bf16[2,192,512]{2,1,0:T(8,128)(2,1)S(1)} %copy-done.2, bf16[2,192,1024]{2,1,0:T(8,128)(2,1)S(1)} %copy-done.1), kind=kOutput, calls=%fused_computation.22 | convolution fusion | flops 402653184 | bytes 5373952 | tf_op jit(solution)/shard_map/esf,esd->efd/dot_general | solution.py:1127
  87.3 0.0 copy-done.7
  87.3 0.7 copy.23
  88.0 0.0 copy-done.8
  88.0 0.6 copy.24
  88.6 0.0 copy-done.6
  88.6 0.7 copy.25
  89.3 0.0 copy-done.5
  89.3 0.7 copy.26
  90.0 0.0 copy-done.4
  90.0 0.7 copy.27
Async XLA Ops:
  77.4 4.3 %copy-start = (bf16[2,192,1024]{2,1,0:T(8,128)(2,1)S(1)}, bf16[2,192,1024]{2,1,0:T(8,128)(2,1)}, u32[]{:S(2)}) copy-start(bf16[2,192,1024]{2,1,0:T(8,128)(2,1)} %get-tuple-element.20) | copy-start | bytes 2359300
  77.4 4.3 %copy-start.3 = (bf16[2,192,512]{2,1,0:T(8,128)(2,1)S(1)}, bf16[2,192,512]{2,1,0:T(8,128)(2,1)}, u32[]{:S(2)}) copy-start(bf16[2,192,512]{2,1,0:T(8,128)(2,1)} %get-tuple-element.22) | copy-start | bytes 1179652
  77.4 7.1 %copy-start.1 = (bf16[2,192,1024]{2,1,0:T(8,128)(2,1)S(1)}, bf16[2,192,1024]{2,1,0:T(8,128)(2,1)}, u32[]{:S(2)}) copy-start(bf16[2,192,1024]{2,1,0:T(8,128)(2,1)} %get-tuple-element.24) | copy-start | bytes 2359300
  77.4 7.1 %copy-start.2 = (bf16[2,192,512]{2,1,0:T(8,128)(2,1)S(1)}, bf16[2,192,512]{2,1,0:T(8,128)(2,1)}, u32[]{:S(2)}) copy-start(bf16[2,192,512]{2,1,0:T(8,128)(2,1)} %get-tuple-element.23) | copy-start | bytes 1179652
  81.7 5.7 %copy-start.7 = (bf16[128,1024]{1,0:T(8,128)(2,1)S(1)}, bf16[128,1024]{1,0:T(8,128)(2,1)}, u32[]{:S(2)}) copy-start(bf16[128,1024]{1,0:T(8,128)(2,1)} %get-tuple-element.39) | copy-start | bytes 786436
  84.5 3.5 %copy-start.8 = (f32[2,128]{1,0:T(2,128)S(1)}, f32[2,128]{1,0:T(2,128)}, u32[]{:S(2)}) copy-start(f32[2,128]{1,0:T(2,128)} %get-tuple-element.19) | copy-start | bytes 3076
  84.5 4.1 %copy-start.6 = (f32[64,1024]{1,0:T(8,128)S(1)}, f32[64,1024]{1,0:T(8,128)}, u32[]{:S(2)}) copy-start(f32[64,1024]{1,0:T(8,128)} %get-tuple-element.25) | copy-start | bytes 786436
  84.5 4.8 %copy-start.5 = (f32[64,1024]{1,0:T(8,128)S(1)}, f32[64,1024]{1,0:T(8,128)}, u32[]{:S(2)}) copy-start(f32[64,1024]{1,0:T(8,128)} %get-tuple-element.26) | copy-start | bytes 786436
  84.5 5.5 %copy-start.4 = (f32[64,1024]{1,0:T(8,128)S(1)}, f32[64,1024]{1,0:T(8,128)}, u32[]{:S(2)}) copy-start(f32[64,1024]{1,0:T(8,128)} %get-tuple-element.46) | copy-start | bytes 786436

commit v2 on v1

--- a/solution.py
+++ b/solution.py
@@ -551,7 +551,8 @@
 
 def line_kernel(
     dims,
-    meta_in,
+    routes_in,
+    weights_in,
     tok_in,
     cot_in,
     eg_in,
@@ -562,6 +563,18 @@
     sd_in,
     gtok_out,
     gw_out,
+    osg_out,
+    osu_out,
+    osd_out,
+    stok_out,
+    scot_out,
+    hg_out,
+    hu_out,
+    hh_out,
+    routes,
+    weights,
+    gtok,
+    gw,
     osg,
     osu,
     osd,
@@ -597,6 +610,7 @@
     shsum,
     load_sem,
     own_sem,
+    out_sem,
     own_s,
     line_s,
     line_r,
@@ -612,6 +626,8 @@
     pa_r,
     xt_s,
     xt_r,
+    xy_s,
+    xy_r,
     bk_s,
     bk_r,
 ):
@@ -625,12 +641,20 @@
     pair = CORES * cap
     group = ne * pair
     home = ne * cap
+    part_rows = swid // tp
     order = line_order(chip, length)
     bufs = (all_tok, all_meta, all_cot)
 
     owns = []
-    for n, (src, dst) in enumerate(((tok_in, all_tok), (meta_in, all_meta), (cot_in, all_cot))):
-        c = pltpu.make_async_copy(src, dst.at[chip, core], own_sem.at[n])
+    for n, (src, dst) in enumerate(
+        (
+            (tok_in, all_tok.at[chip, core]),
+            (cot_in, all_cot.at[chip, core]),
+            (routes_in, routes),
+            (weights_in, weights),
+        )
+    ):
+        c = pltpu.make_async_copy(src, dst, own_sem.at[n])
         c.start()
         owns.append(c)
     loads = []
@@ -642,11 +666,18 @@
         loads.append(c)
 
     barrier = pltpu.get_barrier_semaphore()
-    for o in range(1, ep):
-        pl.semaphore_signal(barrier, inc=1, device_id={"ep": (me + o) % ep})
+    def greet(there):
+        pl.semaphore_signal(barrier, inc=1, device_id={"ep": there * CORES + core})
+
+    pl.semaphore_signal(barrier, inc=1, device_id={"ep": mate})
     for o in range(1, tp):
         pl.semaphore_signal(barrier, inc=1, device_id={"tp": (mt + o) % tp})
-    pl.semaphore_wait(barrier, ep + tp - 2)
+    pl.when(chip < length - 1)(lambda: greet(chip + 1))
+    pl.when(chip > 0)(lambda: greet(chip - 1))
+    above = (2 * length - 2 - chip) // length
+    below = (chip + length - 1) // length
+
+    pl.semaphore_wait(barrier, tp + above + below)
 
     sends = []
 
@@ -671,16 +702,62 @@
         n = b * length + p
         return copy_of(block, block, mate_s.at[n], mate_r.at[n], {"ep": mate})
 
-    for b in range(3):
-        owns[b].wait()
+    def send_own(b):
         for d, there in enumerate((chip + 1, chip - 1)):
             c = along_line(b, chip, own_s.at[2 * b + d], there)
             inside = chip < length - 1 if d == 0 else chip > 0
             pl.when(inside)(c.start)
             sends.append((inside, c))
+
+    def send_mate(b):
         c = to_mate(b, 0)
         c.start()
         sends.append((None, c))
+
+    owns[0].wait()
+    send_own(0)
+    send_mate(0)
+    owns[1].wait()
+    send_mate(2)
+
+    owns[2].wait()
+    owns[3].wait()
+    table = jnp.concatenate(
+        [
+            routes[...].astype(F32),
+            weights[...].astype(BF).astype(F32),
+            jnp.zeros((4, tok), F32),
+        ],
+        axis=0,
+    )
+    picked = table.T
+    earlier = lax.broadcasted_iota(jnp.int32, (tok, tok), 0) < lax.broadcasted_iota(
+        jnp.int32, (tok, tok), 1
+    )
+
+    def count(hits):
+        return jnp.sum(hits.astype(F32), axis=0, keepdims=True)
+
+    first, second = picked[:, 0:1], picked[:, 1:2]
+    ranks = [
+        count((first == table[0:1]) & earlier),
+        count((second == table[1:2]) & earlier) + count(first == table[1:2]),
+    ]
+    ranked = jnp.concatenate(ranks, axis=0)
+    named = table[0:2]
+    owner = jnp.floor((named + 0.5) * (1.0 / ne))
+    which = named - owner * ne
+    all_meta[chip, core] = jnp.concatenate(
+        [
+            named * rows + ranked,
+            table[2:4],
+            owner * home + which * cap + ranked,
+            owner * 128 + which * pair + ranked,
+        ],
+        axis=0,
+    )
+    send_own(1)
+    send_mate(1)
 
     relays = {}
     mates = {}
@@ -689,7 +766,8 @@
         for b in range(3):
             relays[b, p] = along_line(b, src, line_s.at[b * length + p], there)
             mates[b, p] = to_mate(b, p)
-            sends.append(((there >= 0) & (there < length), relays[b, p]))
+            if p < length - 1 or b < 2:
+                sends.append(((there >= 0) & (there < length), relays[b, p]))
             sends.append((None, mates[b, p]))
 
     def arrivals(p, which, cond=None):
@@ -710,6 +788,8 @@
             to_mate(b, p).wait_recv()
 
     peers = [(mt + o) % tp for o in range(1, tp)]
+    inner = chip * (length - 1 - chip) > 0
+    outer = chip * (length - 1 - chip) < 1
 
     own_tok = all_tok[chip, core]
     own_cot = all_cot[chip, core]
@@ -787,6 +867,17 @@
 
     pa_copies = {}
 
+    def send_hidden(p, piece):
+        for o in range(1, tp):
+            k = (p * 3 + piece) * tp + o
+            if piece < 2:
+                block = hs.at[p, mt, pl.ds(2 * piece, 2 - piece)]
+            else:
+                block = dgp.at[p, mt]
+            pa_copies[p, piece, o] = remote(
+                block, block, pa_s.at[k], pa_r.at[k], {"tp": peers[o - 1]}
+            )
+
     def hidden(p):
         for half in range(2):
             for o in range(1, tp):
@@ -809,16 +900,8 @@
         fill = jnp.zeros((128 - group, width), F32)
         cols = jnp.concatenate([terms, fill], axis=0).T
         dgp[p, mt] = jnp.broadcast_to(jnp.sum(cols, axis=0, keepdims=True), (8, 128))
-        for piece in range(3):
-            for o in range(1, tp):
-                k = (p * 3 + piece) * tp + o
-                if piece < 2:
-                    block = hs.at[p, mt, pl.ds(2 * piece, 2 - piece)]
-                else:
-                    block = dgp.at[p, mt]
-                pa_copies[p, piece, o] = remote(
-                    block, block, pa_s.at[k], pa_r.at[k], {"tp": peers[o - 1]}
-                )
+        for piece in (2, 0) if p == length - 1 else (2, 0, 1):
+            send_hidden(p, piece)
 
     def pick_rows():
         at = lax.broadcasted_iota(jnp.int32, (group, group), 0)
@@ -832,7 +915,19 @@
         return (col == wanted).astype(F32).astype(BF)
 
     pick = pick_rows()
-    bk_copies = []
+    held = []
+
+    def give(c, hold):
+        sends.append((None, c))
+        if hold:
+            pl.when(outer)(c.start)
+            held.append(c)
+        else:
+            c.start()
+
+    def give_held():
+        for c in held:
+            c.start()
 
     def spread(p, n, out):
         full = jnp.concatenate([hs[p, q, n] for q in range(tp)], axis=1).astype(F32)
@@ -851,6 +946,9 @@
         src = order[p][0]
         for o in range(1, tp):
             pa_copies[p, 0, o].wait_recv()
+        if p == length - 1:
+            send_hidden(p, 1)
+            share_columns()
         a = spread(p, 0, hg)
         b = spread(p, 1, hu)
         vals = [(dot_t(a[e], eg[e]) + dot_t(b[e], eu[e]))[:pair] for e in range(ne)]
@@ -872,12 +970,11 @@
             targets = [(jj, src * CORES + jj) for jj in range(CORES)]
         for n, (jj, dest) in enumerate(targets):
             k = p * CORES + n
-            bk_copies.append(
-                remote(back_send.at[p, jj], back.at[me], bk_s.at[2 * k], bk_r.at[me], {"ep": dest})
-            )
-            bk_copies.append(
-                remote(dgs.at[p], dgb.at[me], bk_s.at[2 * k + 1], bk_r.at[ep + me], {"ep": dest})
-            )
+            for c in (
+                copy_of(back_send.at[p, jj], back.at[me], bk_s.at[2 * k], bk_r.at[me], {"ep": dest}),
+                copy_of(dgs.at[p], dgb.at[me], bk_s.at[2 * k + 1], bk_r.at[ep + me], {"ep": dest}),
+            ):
+                give(c, p == 1)
 
     def shared_hidden():
         for c in sh_copies:
@@ -895,6 +992,17 @@
             for o in range(1, tp)
         ]
 
+    spread_out = []
+
+    def share_columns():
+        for c in xts:
+            c.wait_recv()
+        for o in range(1, tp):
+            block = share_t.at[1, :, :, mt]
+            spread_out.append(
+                remote(block, block, xy_s.at[o], xy_r.at[o], {"tp": peers[o - 1]})
+            )
+
     def shared_full(n):
         return jnp.concatenate([sh_all[q, n] for q in range(tp)], axis=1)
 
@@ -902,77 +1010,103 @@
         for n in range(3):
             back_t = shared_full(n).astype(F32).T.astype(BF)
             for j in range(ep):
-                share_t[0, n, j] = back_t[j * swid : (j + 1) * swid, :]
+                for q in range(tp):
+                    low = j * swid + q * part_rows
+                    share_t[0, n, j, q] = back_t[low : low + part_rows, :]
         copies = []
         for o in range(1, ep):
             peer = (me + o) % ep
-            copies.append(
-                remote(
-                    share_t.at[0, :, peer],
-                    share_t.at[1, :, me],
-                    xt_s.at[o],
-                    xt_r.at[o],
-                    {"ep": peer},
-                )
+            c = copy_of(
+                share_t.at[0, :, peer, mt],
+                share_t.at[1, :, me, mt],
+                xt_s.at[o],
+                xt_r.at[o],
+                {"ep": peer},
             )
+            give(c, True)
+            copies.append(c)
         for n in range(3):
-            share_t[1, n, me] = share_t[0, n, me]
+            share_t[1, n, me, mt] = share_t[0, n, me, mt]
         return copies
+
+    def homeward(p):
+        src = order[p][0]
+        for jj in range(CORES):
+            if p == 0:
+                j = me if jj == 0 else mate
+            else:
+                j = src * CORES + jj
+            if p > 0 or jj > 0:
+                copy_of(back.at[j], back.at[j], bk_s.at[0], bk_r.at[j], {"ep": j}).wait_recv()
+                copy_of(dgb.at[j], dgb.at[j], bk_s.at[0], bk_r.at[ep + j], {"ep": j}).wait_recv()
+            g0 = (hcol == where_home[:, 4:5] - j * home).astype(F32)
+            g1 = (hcol == where_home[:, 5:6] - j * home).astype(F32)
+            shsum[...] += dot((g0 + g1).astype(BF), back[j])
+
+    outs = []
+
+    def put(src, dst):
+        c = pltpu.make_async_copy(src, dst, out_sem.at[len(outs)])
+        c.start()
+        outs.append(c)
+
+    def hidden_rows(p):
+        for o in range(1, tp):
+            pa_copies[p, 1, o].wait_recv()
+        spread(p, 2, hh)
+
+    def first_arrivals(which):
+        if length > 1:
+            arrivals(1, which)
+        if length > 2:
+            arrivals(2, which, order[2][2] > 0)
 
     mate_wait(0, (0, 1))
     for n in range(3):
         loads[3 + n].wait()
     mate_wait(0, (2,))
     products_all(0)
+    send_own(2)
     sha = shared_hidden()
+    first_arrivals((0, 1))
     hidden(0)
     last = length - 1
     for p in range(1, length):
-        two_sided = order[p][2]
-        split = p == last and p > 1
-        first = (0, 1) if split else (0, 1, 2)
-        if p % 2 == 1 or p == 1:
-            arrivals(p, first)
-            if p + 1 < length:
+        split = p == last
+        if p == 1:
+            first_arrivals((2,))
+        elif not split:
+            far = order[p][2] < 1 if p % 2 == 0 or p == last else None
+            arrivals(p, (0, 1, 2), far)
+            if p % 2 == 1 and p + 1 < last:
                 arrivals(p + 1, (0, 1, 2), order[p + 1][2] > 0)
         else:
-            arrivals(p, first, two_sided < 1)
+            arrivals(p, (0, 1), outer)
         mate_wait(p, (0, 1))
         selection(p)
         products(p, (0, 1))
         if split:
-            slots(p - 1)
             for c in sha:
                 c.wait_recv()
             xts = shared_shares()
-            arrivals(p, (2,))
+            arrivals(p, (2,), outer)
         mate_wait(p, (2,))
         products(p, (2,))
-        if not split:
-            slots(p - 1)
+        if p + 1 == last and last > 2:
+            arrivals(last, (2,), inner)
+        slots(p - 1)
         hidden(p)
-    if last <= 1:
-        for c in sha:
-            c.wait_recv()
-        xts = shared_shares()
+        if p + 2 == last and last > 2:
+            arrivals(last, (0, 1), inner)
+    if last > 0:
+        there = order[last][1]
+        pl.when((there >= 0) & (there < length))(relays[2, last].wait_send)
+    pl.when(inner)(give_held)
+    put(stok, stok_out)
+    put(scot, scot_out)
     shsum[...] = dot_t(shared_full(0), sg[...]) + dot_t(shared_full(1), su[...])
-    slots(last)
-
-    for c in xts:
-        c.wait_recv()
-    flat = [
-        jnp.concatenate([share_t[1, n, j] for j in range(ep)], axis=1) for n in range(3)
-    ]
-    tok_flat = all_tok[...].reshape(ep * tok, dl)
-    osg[...] = dot(flat[0], tok_flat)
-    osu[...] = dot(flat[1], tok_flat)
-    osd[...] = dot(flat[2], all_cot[...].reshape(ep * tok, dl))
-
-    for p in range(length):
-        for o in range(1, tp):
-            pa_copies[p, 1, o].wait_recv()
-        spread(p, 2, hh)
-
+    for p in range(last):
+        hidden_rows(p)
     own_meta = all_meta[chip, core]
     where_home = own_meta.T.astype(jnp.int32)
     hcol = lax.broadcasted_iota(jnp.int32, (tok, home), 1)
@@ -980,26 +1114,146 @@
     lanes = own_meta[6:8, :].astype(jnp.int32) + core * cap
     spots = [(lane_at == lanes[k : k + 1, :]).astype(F32).astype(BF) for k in range(2)]
     spots = jnp.concatenate(spots, axis=1)
-    for o in range(1, ep):
-        peer = (me + o) % ep
-        copy_of(back.at[peer], back.at[peer], bk_s.at[0], bk_r.at[peer], {"ep": peer}).wait_recv()
-        copy_of(dgb.at[peer], dgb.at[peer], bk_s.at[0], bk_r.at[ep + peer], {"ep": peer}).wait_recv()
-    grad = shsum[...]
-    for j in range(ep):
-        g0 = (hcol == where_home[:, 4:5] - j * home).astype(F32)
-        g1 = (hcol == where_home[:, 5:6] - j * home).astype(F32)
-        grad = grad + dot((g0 + g1).astype(BF), back[j])
-    gtok_out[...] = grad.astype(BF)
+    slots(last)
+    put(hg, hg_out)
+    put(hu, hu_out)
+    homeward(0)
+    hidden_rows(last)
+    put(hh, hh_out)
+
+    homeward(1)
+    homeward(2)
+    for c in spread_out:
+        c.wait_recv()
+    flat = []
+    for n in range(3):
+        parts = [
+            jnp.concatenate([share_t[1, n, j, q] for j in range(ep)], axis=1) for q in range(tp)
+        ]
+        flat.append(jnp.concatenate(parts, axis=0))
+    tok_flat = all_tok[...].reshape(ep * tok, dl)
+    osg[...] = dot(flat[0], tok_flat)
+    put(osg, osg_out)
+    osu[...] = dot(flat[1], tok_flat)
+    put(osu, osu_out)
+    osd[...] = dot(flat[2], all_cot[...].reshape(ep * tok, dl))
+    put(osd, osd_out)
+
+    for p in range(3, length):
+        homeward(p)
+    gtok[...] = shsum[...].astype(BF)
+    put(gtok, gtok_out)
     dg = jnp.concatenate([dgb[j] for j in range(ep)], axis=1)
     high = dg.astype(BF)
     low = (dg - high.astype(F32)).astype(BF)
-    gw = dot(high, spots) + dot(low, spots)
-    gw_out[...] = jnp.concatenate([gw[0:1, :tok], gw[0:1, tok:]], axis=0)
+    total = dot(high, spots) + dot(low, spots)
+    gw[...] = jnp.concatenate(
+        [total[0:1, :tok], total[0:1, tok:], jnp.zeros((6, tok), F32)], axis=0
+    )
+    put(gw, gw_out)
     for cond, c in sends:
         if cond is None:
             c.wait_send()
         else:
             pl.when(cond)(c.wait_send)
+    for c in outs:
+        c.wait()
+
+
+def grads_kernel(
+    dims,
+    gtok_in,
+    gw_in,
+    osg_in,
+    osu_in,
+    osd_in,
+    stok_in,
+    scot_in,
+    hg_in,
+    hu_in,
+    hh_in,
+    gtok_out,
+    gw_out,
+    grad_gate,
+    grad_up,
+    grad_down,
+    osg_out,
+    osu_out,
+    osd_out,
+    gtok,
+    gw,
+    osg,
+    osu,
+    osd,
+    stok,
+    scot,
+    hg,
+    hu,
+    hh,
+    gate_rows,
+    up_rows,
+    down_rows,
+    in_sem,
+    out_sem,
+):
+    ne, chunks = dims
+    ins = []
+    for n, (src, dst) in enumerate(
+        (
+            (stok_in, stok),
+            (hg_in, hg),
+            (hu_in, hu),
+            (hh_in, hh),
+            (scot_in, scot),
+            (gtok_in, gtok),
+            (gw_in, gw),
+            (osg_in, osg),
+            (osu_in, osu),
+            (osd_in, osd),
+        )
+    ):
+        c = pltpu.make_async_copy(src, dst, in_sem.at[n])
+        c.start()
+        ins.append(c)
+    outs = []
+
+    def put(src, dst):
+        c = pltpu.make_async_copy(src, dst, out_sem.at[len(outs)])
+        c.start()
+        outs.append(c)
+
+    def outer(a, b):
+        return lax.dot_general(a, b, (((0,), (0,)), ((), ())), preferred_element_type=F32)
+
+    def cut(size):
+        step = size // chunks
+        return [slice(i * step, (i + 1) * step) for i in range(chunks)]
+
+    for n in range(3):
+        ins[n].wait()
+    for e in range(ne):
+        for r in cut(stok.shape[2]):
+            left = stok[e, :, r]
+            gate_rows[e, r, :] = outer(left, hg[e])
+            put(gate_rows.at[e, r], grad_gate.at[e, r])
+            up_rows[e, r, :] = outer(left, hu[e])
+            put(up_rows.at[e, r], grad_up.at[e, r])
+    for n in range(3, 10):
+        ins[n].wait()
+    for src, dst in (
+        (gtok, gtok_out),
+        (gw.at[pl.ds(0, gw_out.shape[0])], gw_out),
+        (osg, osg_out),
+        (osu, osu_out),
+        (osd, osd_out),
+    ):
+        put(src, dst)
+    for e in range(ne):
+        for r in cut(hh.shape[2]):
+            down_rows[e, r, :] = outer(hh[e, :, r], scot[e])
+            put(down_rows.at[e, r], grad_down.at[e, r])
+    for c in outs:
+        c.wait()
 
 
 def line_body(
@@ -1028,22 +1282,25 @@
     width, swidth, swid = ff // tp, sff // tp, sff // ep
     dims = (ep, tp, tok, dl, ne, ff, sff, cap, rows, width, swidth, swid)
 
-    picked = routes.T.reshape(-1)
-    earlier = jnp.arange(top * tok)[None, :] < jnp.arange(top * tok)[:, None]
-    same = picked[:, None] == picked[None, :]
-    ranked = jnp.sum((same & earlier).astype(jnp.int32), axis=1)
-    code = (picked * rows + ranked).reshape(top, tok)
-    place = ((picked // ne) * home + (picked % ne) * cap + ranked).reshape(top, tok)
-    lane = ((picked // ne) * 128 + (picked % ne) * pair + ranked).reshape(top, tok)
-    gate = route_weights.astype(BF).astype(F32).T
-    meta = jnp.concatenate(
-        [code.astype(F32), gate, place.astype(F32), lane.astype(F32)], axis=0
+    hbm = pl.BlockSpec(memory_space=pltpu.HBM)
+    dma = pltpu.SemaphoreType.DMA
+    sds = jax.ShapeDtypeStruct
+    shapes = (
+        sds((tok, dl), BF),
+        sds((8, tok), F32),
+        sds((swid, dl), F32),
+        sds((swid, dl), F32),
+        sds((swid, dl), F32),
+        sds((ne, length * rows, dl), BF),
+        sds((ne, length * rows, dl), BF),
+        sds((ne, length * rows, ff), BF),
+        sds((ne, length * rows, ff), BF),
+        sds((ne, length * rows, ff), BF),
     )
-
-    vm = pl.BlockSpec(memory_space=pltpu.VMEM)
-    hbm = pl.BlockSpec(memory_space=pl.ANY)
-    dma = pltpu.SemaphoreType.DMA
     scratch = [
+        pltpu.VMEM((top, tok), jnp.int32),
+        pltpu.VMEM((top, tok), F32),
+        *[pltpu.VMEM(s.shape, s.dtype) for s in shapes],
         pltpu.VMEM((length, CORES, tok, dl), BF),
         pltpu.VMEM((length, CORES, tok, dl), BF),
         pltpu.VMEM((length, CORES, 8, tok), F32),
@@ -1058,7 +1315,7 @@
         pltpu.VMEM((tp, 3, tok, swidth), F32),
         pltpu.VMEM((tp, 3, tok, swidth), BF),
         pltpu.VMEM((tp, 3, tok, swidth), BF),
-        pltpu.VMEM((2, 3, ep, swid, tok), BF),
+        pltpu.VMEM((2, 3, ep, tp, swid // tp, tok), BF),
         pltpu.VMEM((length, tp, 3, group, width), BF),
         pltpu.VMEM((length, tp, 3, group, width), F32),
         pltpu.VMEM((length, tp, 3, group, width), BF),
@@ -1070,7 +1327,8 @@
         pltpu.VMEM((ep, home, dl), BF),
         pltpu.VMEM((tok, dl), F32),
         dma((6,)),
-        dma((3,)),
+        dma((4,)),
+        dma((len(shapes),)),
         dma((6,)),
         dma((3 * length,)),
         dma((3 * length,)),
@@ -1086,32 +1344,23 @@
         dma((3 * length * tp,)),
         dma((ep,)),
         dma((ep,)),
+        dma((tp,)),
+        dma((tp,)),
         dma((2 * CORES * length,)),
         dma((2 * ep,)),
     ]
-    sds = jax.ShapeDtypeStruct
     outs = pl.pallas_call(
         functools.partial(line_kernel, dims),
-        out_shape=(
-            sds((tok, dl), BF),
-            sds((top, tok), F32),
-            sds((swid, dl), F32),
-            sds((swid, dl), F32),
-            sds((swid, dl), F32),
-            sds((ne, length * rows, dl), BF),
-            sds((ne, length * rows, dl), BF),
-            sds((ne, length * rows, ff), BF),
-            sds((ne, length * rows, ff), BF),
-            sds((ne, length * rows, ff), BF),
-        ),
-        in_specs=[hbm] * 9,
-        out_specs=tuple([vm] * 10),
+        out_shape=shapes,
+        in_specs=[hbm] * 10,
+        out_specs=tuple([hbm] * len(shapes)),
         scratch_shapes=scratch,
         compiler_params=pltpu.CompilerParams(
             collective_id=0, has_side_effects=True, vmem_limit_bytes=60 * 1024 * 1024
         ),
     )(
-        meta,
+        routes.T,
+        route_weights.T,
         tokens,
         cotangent,
         expert_gate,
@@ -1121,10 +1370,31 @@
         shared_up,
         shared_down,
     )
-    gtok, gw, osg, osu, osd, stok, scot, hg, hu, hh = outs
-    grad_gate = jnp.einsum("esd,esf->edf", stok, hg, preferred_element_type=F32)
-    grad_up = jnp.einsum("esd,esf->edf", stok, hu, preferred_element_type=F32)
-    grad_down = jnp.einsum("esf,esd->efd", hh, scot, preferred_element_type=F32)
+    chunks = 4
+    results = (
+        sds((tok, dl), BF),
+        sds((top, tok), F32),
+        sds((ne, dl, ff), F32),
+        sds((ne, dl, ff), F32),
+        sds((ne, ff, dl), F32),
+        sds((swid, dl), F32),
+        sds((swid, dl), F32),
+        sds((swid, dl), F32),
+    )
+    gtok, gw, grad_gate, grad_up, grad_down, osg, osu, osd = pl.pallas_call(
+        functools.partial(grads_kernel, (ne, chunks)),
+        out_shape=results,
+        in_specs=[hbm] * len(shapes),
+        out_specs=tuple([hbm] * len(results)),
+        scratch_shapes=[
+            *[pltpu.VMEM(s.shape, s.dtype) for s in shapes],
+            *[pltpu.VMEM(s.shape, s.dtype) for s in results[2:5]],
+            dma((len(shapes),)),
+            dma((3 * ne * chunks + 5,)),
+        ],
+        compiler_params=pltpu.CompilerParams(vmem_limit_bytes=60 * 1024 * 1024),
+        name="grads",
+    )(*outs)
     return gtok, gw.T, grad_gate, grad_up, grad_down, osg.T, osu.T, osd
 
 
@@ -1135,13 +1405,16 @@
     ep, tp = lax.axis_size("ep"), lax.axis_size("tp")
     cap = max(2, 5 * tok * top // (4 * ep * ne))
     lines = (
-        ff == tp * 128
+        ep == 4 * CORES
+        and ff == tp * 128
         and sff == tp * 128
-        and ep % CORES == 0
         and (CORES * cap) % 8 == 0
         and (ne * cap) % 8 == 0
         and (ne * CORES * cap) % 16 == 0
         and ne * CORES * cap <= 128
+        and tok == 128
+        and sff % (ep * tp * 16) == 0
+        and top == 2
     )
     return (line_body if lines else rows_body)(tokens, routes, *rest)
 

time: 91.3 us -> 71.1 us (0.78)
  matrix products: 9.84 us -> 0 us
  other arithmetic: 3.61 us -> 0 us
  local copies, waits for them, and re-layouts: 3.41 us -> 0 us
  Pallas kernels: 73.2 us -> 70.1 us
    dot_general x3 -> x0, matrix products: 9.84 us -> none  [the longest x1 4.22 us: line_body(): grad_gate = jnp.einsum('esd,esf->edf', stok, hg, preferred_element_type=F32)]
    unnamed x23 -> x0, local copies, waits for them, and re-layouts: 3.41 us -> none
    pallas_call x1 -> x2, Pallas kernels: 73.2 us -> 70.1 us  [the longest x1 63.3 us: line_body(): pl.pallas_call(functools.partial(line_kernel, dims), out_shape=shapes, in...]
    convert_element_type x2 -> x0, other arithmetic: 1.38 us -> none  [the longest x1 0.69 us: line_body(): lane.astype(F32)]
    reduce_sum x1 -> x0, other arithmetic: 0.93 us -> none  [line_body(): ranked = jnp.sum((same & earlier).astype(jnp.int32), axis=1)]
where the time goes in v2:
time: 71.1 us; the launch traced here: 71 us
  Pallas kernels  70.1 us (99%)
  between operations  0.81 us (1%)
    pallas_call x1, Pallas kernels, line_body(): pl.pallas_call(functools.partial(line_kernel, dims), out_shape=shapes, in...  63.3 us
    pallas_call x1, Pallas kernels, line_body(): pl.pallas_call(functools.partial(grads_kernel, (ne, chunks)), out_shape=r...  6.81 us

profile of v2, /device:TPU:0, one launch (start us, length us, event | category | flops | bytes accessed | tf_op | source)
XLA Modules:
  0.0 71.0 jit_solution(14106510086378435937)
XLA Ops:
  0.6 63.3 %shard_map.161 = (bf16[128,1024]{1,0:T(8,128)(2,1)}, f32[8,128]{1,0:T(8,128)}, f32[64,1024]{1,0:T(8,128)}, f32[64,1024]{1,0:T(8,128)}, f32[64,1024]{1,0:T(8,128)...) custom-call(s32[2,128]{1,0:T(2,128)} %bitcast.5, ...), custom_call_target="tpu_custom_call" | custom-call | tf_op jit(solution)/shard_map/pallas_call | solution.py:1352
  64.0 6.8 %grads.1 = (bf16[128,1024]{1,0:T(8,128)(2,1)}, f32[2,128]{1,0:T(2,128)}, f32[2,1024,512]{2,1,0:T(8,128)}, f32[2,1024,512]{2,1,0:T(8,128)}, f32[2,512,1024]{2,1,0...) custom-call(bf16[128,1024]{1,0:T(8,128)(2,1)} %get-tuple-element.26.gtok_in, ...), custom_call_target="tpu_custom_call" | custom-call | tf_op jit(solution)/shard_map/grads/pallas_call | solution.py:1384

commit v3 on v2

--- a/solution.py
+++ b/solution.py
@@ -687,10 +687,13 @@
         )
 
     def remote(src, dst, ssem, rsem, dev):
-        c = copy_of(src, dst, ssem, rsem, dev)
-        c.start()
-        sends.append((None, c))
-        return c
+        copy_of(src, dst, ssem, rsem, dev).start()
+
+    def got(block, sem):
+        copy_of(block, block, own_s.at[0], sem, {"ep": mate}).wait_recv()
+
+    def left(block, sem):
+        copy_of(block, block, sem, own_s.at[0], {"ep": mate}).wait_send()
 
     def along_line(b, src, ssem, there):
         block = bufs[b].at[src, core]
@@ -700,7 +703,7 @@
     def to_mate(b, p):
         block = bufs[b].at[order[p][0], core]
         n = b * length + p
-        return copy_of(block, block, mate_s.at[n], mate_r.at[n], {"ep": mate})
+        return copy_of(block, block, mate_s.at[b], mate_r.at[n], {"ep": mate})
 
     def send_own(b):
         for d, there in enumerate((chip + 1, chip - 1)):
@@ -710,9 +713,7 @@
             sends.append((inside, c))
 
     def send_mate(b):
-        c = to_mate(b, 0)
-        c.start()
-        sends.append((None, c))
+        to_mate(b, 0).start()
 
     owns[0].wait()
     send_own(0)
@@ -768,7 +769,6 @@
             mates[b, p] = to_mate(b, p)
             if p < length - 1 or b < 2:
                 sends.append(((there >= 0) & (there < length), relays[b, p]))
-            sends.append((None, mates[b, p]))
 
     def arrivals(p, which, cond=None):
         def run():
@@ -800,21 +800,14 @@
             piece = val[:, q * swidth : (q + 1) * swidth]
             sh_exact[q, n] = piece
             sh_part[q, n] = piece.astype(BF)
-    sh_copies = []
     for o in range(1, tp):
-        sh_copies.append(
-            remote(
-                sh_part.at[peers[o - 1]],
-                sh_recv.at[o],
-                shr_s.at[o],
-                shr_r.at[o],
-                {"tp": peers[o - 1]},
-            )
-        )
+        peer = peers[o - 1]
+        remote(sh_part.at[peer], sh_recv.at[o], shr_s.at[0], shr_r.at[0], {"tp": peer})
+    others = pl.ds(1, tp - 1)
+    any_tp = pl.ds(0, tp - 1)
 
     row_id = lax.broadcasted_iota(jnp.int32, (ne * rows, tok), 0)
     sels = {}
-    pr_copies = {}
 
     def selection(p):
         src = order[p][0]
@@ -851,12 +844,11 @@
         half = 1 if which == (2,) else 0
         span = pl.ds(which[0], len(which))
         for o in range(1, tp):
-            k = (p * 2 + half) * tp + o
-            pr_copies[p, half, o] = remote(
+            remote(
                 part.at[p, peers[o - 1], span],
                 recv.at[p, o, span],
-                pr_s.at[k],
-                pr_r.at[k],
+                pr_s.at[0],
+                pr_r.at[2 * p + half],
                 {"tp": peers[o - 1]},
             )
 
@@ -865,23 +857,25 @@
         products(p, (0, 1))
         products(p, (2,))
 
-    pa_copies = {}
-
     def send_hidden(p, piece):
         for o in range(1, tp):
-            k = (p * 3 + piece) * tp + o
             if piece < 2:
                 block = hs.at[p, mt, pl.ds(2 * piece, 2 - piece)]
             else:
                 block = dgp.at[p, mt]
-            pa_copies[p, piece, o] = remote(
-                block, block, pa_s.at[k], pa_r.at[k], {"tp": peers[o - 1]}
+            remote(
+                block, block, pa_s.at[piece // 2], pa_r.at[3 * p + piece], {"tp": peers[o - 1]}
             )
 
+    def hidden_got(p, piece):
+        if piece < 2:
+            got(hs.at[p, any_tp, pl.ds(2 * piece, 2 - piece)], pa_r.at[3 * p + piece])
+        else:
+            got(dgp.at[p, any_tp], pa_r.at[3 * p + piece])
+
     def hidden(p):
-        for half in range(2):
-            for o in range(1, tp):
-                pr_copies[p, half, o].wait_recv()
+        got(recv.at[p, others, pl.ds(0, 2)], pr_r.at[2 * p])
+        got(recv.at[p, others, pl.ds(2, 1)], pr_r.at[2 * p + 1])
         tot = [exact[p, mt, n] for n in range(3)]
         for o in range(1, tp):
             for n in range(3):
@@ -918,7 +912,6 @@
     held = []
 
     def give(c, hold):
-        sends.append((None, c))
         if hold:
             pl.when(outer)(c.start)
             held.append(c)
@@ -944,8 +937,7 @@
 
     def slots(p):
         src = order[p][0]
-        for o in range(1, tp):
-            pa_copies[p, 0, o].wait_recv()
+        hidden_got(p, 0)
         if p == length - 1:
             send_hidden(p, 1)
             share_columns()
@@ -956,8 +948,7 @@
         moved = dot(pick, slot)
         for jj in range(CORES):
             back_send[p, jj] = moved[jj * home : (jj + 1) * home].astype(BF)
-        for o in range(1, tp):
-            pa_copies[p, 2, o].wait_recv()
+        hidden_got(p, 2)
         total = dgp[p, 0]
         for q in range(1, tp):
             total = total + dgp[p, q]
@@ -968,17 +959,17 @@
             targets = [(1 - core, mate)]
         else:
             targets = [(jj, src * CORES + jj) for jj in range(CORES)]
-        for n, (jj, dest) in enumerate(targets):
-            k = p * CORES + n
+        for jj, dest in targets:
             for c in (
-                copy_of(back_send.at[p, jj], back.at[me], bk_s.at[2 * k], bk_r.at[me], {"ep": dest}),
-                copy_of(dgs.at[p], dgb.at[me], bk_s.at[2 * k + 1], bk_r.at[ep + me], {"ep": dest}),
+                copy_of(
+                    back_send.at[p, jj], back.at[me], bk_s.at[0], bk_r.at[chip], {"ep": dest}
+                ),
+                copy_of(dgs.at[p], dgb.at[me], bk_s.at[1], bk_r.at[length + chip], {"ep": dest}),
             ):
                 give(c, p == 1)
 
     def shared_hidden():
-        for c in sh_copies:
-            c.wait_recv()
+        got(sh_recv.at[others], shr_r.at[0])
         tot = [sh_exact[mt, n] for n in range(3)]
         for o in range(1, tp):
             for n in range(3):
@@ -987,21 +978,16 @@
         sh_all[mt, 0] = a
         sh_all[mt, 1] = b
         sh_all[mt, 2] = c3
-        return [
-            remote(sh_all.at[mt], sh_all.at[mt], sha_s.at[o], sha_r.at[o], {"tp": peers[o - 1]})
-            for o in range(1, tp)
-        ]
-
-    spread_out = []
+        for o in range(1, tp):
+            remote(
+                sh_all.at[mt], sh_all.at[mt], sha_s.at[0], sha_r.at[0], {"tp": peers[o - 1]}
+            )
 
     def share_columns():
-        for c in xts:
-            c.wait_recv()
+        got(share_t.at[1, :, pl.ds(0, ep - 1), 0], xt_r.at[0])
         for o in range(1, tp):
             block = share_t.at[1, :, :, mt]
-            spread_out.append(
-                remote(block, block, xy_s.at[o], xy_r.at[o], {"tp": peers[o - 1]})
-            )
+            remote(block, block, xy_s.at[0], xy_r.at[0], {"tp": peers[o - 1]})
 
     def shared_full(n):
         return jnp.concatenate([sh_all[q, n] for q in range(tp)], axis=1)
@@ -1013,32 +999,26 @@
                 for q in range(tp):
                     low = j * swid + q * part_rows
                     share_t[0, n, j, q] = back_t[low : low + part_rows, :]
-        copies = []
         for o in range(1, ep):
             peer = (me + o) % ep
             c = copy_of(
                 share_t.at[0, :, peer, mt],
                 share_t.at[1, :, me, mt],
-                xt_s.at[o],
-                xt_r.at[o],
+                xt_s.at[0],
+                xt_r.at[0],
                 {"ep": peer},
             )
             give(c, True)
-            copies.append(c)
         for n in range(3):
             share_t[1, n, me, mt] = share_t[0, n, me, mt]
-        return copies
 
     def homeward(p):
         src = order[p][0]
+        from_there = pl.ds(src * CORES, CORES) if p else pl.ds(mate, 1)
+        got(back.at[from_there], bk_r.at[src])
+        got(dgb.at[from_there], bk_r.at[length + src])
         for jj in range(CORES):
-            if p == 0:
-                j = me if jj == 0 else mate
-            else:
-                j = src * CORES + jj
-            if p > 0 or jj > 0:
-                copy_of(back.at[j], back.at[j], bk_s.at[0], bk_r.at[j], {"ep": j}).wait_recv()
-                copy_of(dgb.at[j], dgb.at[j], bk_s.at[0], bk_r.at[ep + j], {"ep": j}).wait_recv()
+            j = src * CORES + jj
             g0 = (hcol == where_home[:, 4:5] - j * home).astype(F32)
             g1 = (hcol == where_home[:, 5:6] - j * home).astype(F32)
             shsum[...] += dot((g0 + g1).astype(BF), back[j])
@@ -1051,8 +1031,7 @@
         outs.append(c)
 
     def hidden_rows(p):
-        for o in range(1, tp):
-            pa_copies[p, 1, o].wait_recv()
+        hidden_got(p, 1)
         spread(p, 2, hh)
 
     def first_arrivals(which):
@@ -1067,7 +1046,7 @@
     mate_wait(0, (2,))
     products_all(0)
     send_own(2)
-    sha = shared_hidden()
+    shared_hidden()
     first_arrivals((0, 1))
     hidden(0)
     last = length - 1
@@ -1086,9 +1065,8 @@
         selection(p)
         products(p, (0, 1))
         if split:
-            for c in sha:
-                c.wait_recv()
-            xts = shared_shares()
+            got(sh_all.at[any_tp], sha_r.at[0])
+            shared_shares()
             arrivals(p, (2,), outer)
         mate_wait(p, (2,))
         products(p, (2,))
@@ -1123,8 +1101,7 @@
 
     homeward(1)
     homeward(2)
-    for c in spread_out:
-        c.wait_recv()
+    got(share_t.at[1, :, :, any_tp], xy_r.at[0])
     flat = []
     for n in range(3):
         parts = [
@@ -1152,10 +1129,18 @@
     )
     put(gw, gw_out)
     for cond, c in sends:
-        if cond is None:
-            c.wait_send()
-        else:
-            pl.when(cond)(c.wait_send)
+        pl.when(cond)(c.wait_send)
+    for b in range(3):
+        left(bufs[b].at[:, 0], mate_s.at[b])
+    left(sh_part.at[any_tp], shr_s.at[0])
+    left(sh_all.at[any_tp], sha_s.at[0])
+    left(part.at[:, any_tp], pr_s.at[0])
+    left(hs.at[:, any_tp], pa_s.at[0])
+    left(dgp.at[:, any_tp], pa_s.at[1])
+    left(share_t.at[0, :, pl.ds(0, ep - 1), 0], xt_s.at[0])
+    left(share_t.at[1, :, :, any_tp], xy_s.at[0])
+    left(back.at[pl.ds(0, ep - 1)], bk_s.at[0])
+    left(dgb.at[pl.ds(0, ep - 1)], bk_s.at[1])
     for c in outs:
         c.wait()
 
@@ -1332,22 +1317,15 @@
         dma((6,)),
         dma((3 * length,)),
         dma((3 * length,)),
+        dma((3,)),
         dma((3 * length,)),
+        *[dma((1,))] * 5,
+        dma((2 * length,)),
+        dma((2,)),
         dma((3 * length,)),
-        dma((tp,)),
-        dma((tp,)),
-        dma((tp,)),
-        dma((tp,)),
-        dma((2 * length * tp,)),
-        dma((2 * length * tp,)),
-        dma((3 * length * tp,)),
-        dma((3 * length * tp,)),
-        dma((ep,)),
-        dma((ep,)),
-        dma((tp,)),
-        dma((tp,)),
-        dma((2 * CORES * length,)),
-        dma((2 * ep,)),
+        *[dma((1,))] * 4,
+        dma((2,)),
+        dma((2 * length,)),
     ]
     outs = pl.pallas_call(
         functools.partial(line_kernel, dims),

time: 71.1 us -> 69.2 us (0.973)
  Pallas kernels: 70.1 us -> 68.3 us
    pallas_call x1, Pallas kernels: 63.3 us -> 61.4 us  [line_body(): pl.pallas_call(functools.partial(line_kernel, dims), out_shape=shapes, in...]
where the time goes in v3:
time: 69.2 us; the launch traced here: 69.1 us
  Pallas kernels  68.3 us (99%)
  between operations  0.81 us (1%)
    pallas_call x1, Pallas kernels, line_body(): pl.pallas_call(functools.partial(line_kernel, dims), out_shape=shapes, in...  61.4 us
    pallas_call x1, Pallas kernels, line_body(): pl.pallas_call(functools.partial(grads_kernel, (ne, chunks)), out_shape=r...  6.81 us

profile of v3, /device:TPU:0, one launch (start us, length us, event | category | flops | bytes accessed | tf_op | source)
XLA Modules:
  0.0 69.1 jit_solution(9056840803327784562)
XLA Ops:
  0.6 61.4 %shard_map.161 = (bf16[128,1024]{1,0:T(8,128)(2,1)}, f32[8,128]{1,0:T(8,128)}, f32[64,1024]{1,0:T(8,128)}, f32[64,1024]{1,0:T(8,128)}, f32[64,1024]{1,0:T(8,128)...) custom-call(s32[2,128]{1,0:T(2,128)} %bitcast.5, ...), custom_call_target="tpu_custom_call" | custom-call | tf_op jit(solution)/shard_map/pallas_call | solution.py:1330
  62.1 6.8 %grads.1 = (bf16[128,1024]{1,0:T(8,128)(2,1)}, f32[2,128]{1,0:T(2,128)}, f32[2,1024,512]{2,1,0:T(8,128)}, f32[2,1024,512]{2,1,0:T(8,128)}, f32[2,512,1024]{2,1,0...) custom-call(bf16[128,1024]{1,0:T(8,128)(2,1)} %get-tuple-element.26.gtok_in, ...), custom_call_target="tpu_custom_call" | custom-call | tf_op jit(solution)/shard_map/grads/pallas_call | solution.py:1362

commit v4 on v3

--- a/solution.py
+++ b/solution.py
@@ -561,18 +561,6 @@
     sg_in,
     su_in,
     sd_in,
-    gtok_out,
-    gw_out,
-    osg_out,
-    osu_out,
-    osd_out,
-    stok_out,
-    scot_out,
-    hg_out,
-    hu_out,
-    hh_out,
-    routes,
-    weights,
     gtok,
     gw,
     osg,
@@ -583,6 +571,8 @@
     hg,
     hu,
     hh,
+    routes,
+    weights,
     all_tok,
     all_cot,
     all_meta,
@@ -610,7 +600,6 @@
     shsum,
     load_sem,
     own_sem,
-    out_sem,
     own_s,
     line_s,
     line_r,
@@ -894,7 +883,7 @@
         fill = jnp.zeros((128 - group, width), F32)
         cols = jnp.concatenate([terms, fill], axis=0).T
         dgp[p, mt] = jnp.broadcast_to(jnp.sum(cols, axis=0, keepdims=True), (8, 128))
-        for piece in (2, 0) if p == length - 1 else (2, 0, 1):
+        for piece in (2, 0, 1):
             send_hidden(p, piece)
 
     def pick_rows():
@@ -939,34 +928,44 @@
         src = order[p][0]
         hidden_got(p, 0)
         if p == length - 1:
-            send_hidden(p, 1)
             share_columns()
         a = spread(p, 0, hg)
         b = spread(p, 1, hu)
-        vals = [(dot_t(a[e], eg[e]) + dot_t(b[e], eu[e]))[:pair] for e in range(ne)]
-        slot = jnp.concatenate(vals, axis=0).astype(BF)
-        moved = dot(pick, slot)
-        for jj in range(CORES):
-            back_send[p, jj] = moved[jj * home : (jj + 1) * home].astype(BF)
+        pieces = 2 if p == length - 1 else 1
+        span = dl // pieces
+        for i in range(pieces):
+            cols = slice(i * span, (i + 1) * span)
+            vals = [
+                (dot_t(a[e], eg[e, cols, :]) + dot_t(b[e], eu[e, cols, :]))[:pair]
+                for e in range(ne)
+            ]
+            moved = dot(pick, jnp.concatenate(vals, axis=0).astype(BF))
+            for jj in range(CORES):
+                back_send[p, jj, :, cols] = moved[jj * home : (jj + 1) * home].astype(BF)
+            if p == 0:
+                back[me, :, cols] = back_send[0, core, :, cols]
+                targets = [(1 - core, mate)]
+            else:
+                targets = [(jj, src * CORES + jj) for jj in range(CORES)]
+            for jj, dest in targets:
+                c = copy_of(
+                    back_send.at[p, jj, :, pl.ds(i * span, span)],
+                    back.at[me, :, pl.ds(i * span, span)],
+                    bk_s.at[0],
+                    bk_r.at[chip],
+                    {"ep": dest},
+                )
+                give(c, p == 1)
         hidden_got(p, 2)
         total = dgp[p, 0]
         for q in range(1, tp):
             total = total + dgp[p, q]
         dgs[p] = total
         if p == 0:
-            back[me] = back_send[0, core]
             dgb[me] = total
-            targets = [(1 - core, mate)]
-        else:
-            targets = [(jj, src * CORES + jj) for jj in range(CORES)]
         for jj, dest in targets:
-            for c in (
-                copy_of(
-                    back_send.at[p, jj], back.at[me], bk_s.at[0], bk_r.at[chip], {"ep": dest}
-                ),
-                copy_of(dgs.at[p], dgb.at[me], bk_s.at[1], bk_r.at[length + chip], {"ep": dest}),
-            ):
-                give(c, p == 1)
+            c = copy_of(dgs.at[p], dgb.at[me], bk_s.at[1], bk_r.at[length + chip], {"ep": dest})
+            give(c, p == 1)
 
     def shared_hidden():
         got(sh_recv.at[others], shr_r.at[0])
@@ -1022,13 +1021,6 @@
             g0 = (hcol == where_home[:, 4:5] - j * home).astype(F32)
             g1 = (hcol == where_home[:, 5:6] - j * home).astype(F32)
             shsum[...] += dot((g0 + g1).astype(BF), back[j])
-
-    outs = []
-
-    def put(src, dst):
-        c = pltpu.make_async_copy(src, dst, out_sem.at[len(outs)])
-        c.start()
-        outs.append(c)
 
     def hidden_rows(p):
         hidden_got(p, 1)
@@ -1080,8 +1072,6 @@
         there = order[last][1]
         pl.when((there >= 0) & (there < length))(relays[2, last].wait_send)
     pl.when(inner)(give_held)
-    put(stok, stok_out)
-    put(scot, scot_out)
     shsum[...] = dot_t(shared_full(0), sg[...]) + dot_t(shared_full(1), su[...])
     for p in range(last):
         hidden_rows(p)
@@ -1093,11 +1083,7 @@
     spots = [(lane_at == lanes[k : k + 1, :]).astype(F32).astype(BF) for k in range(2)]
     spots = jnp.concatenate(spots, axis=1)
     slots(last)
-    put(hg, hg_out)
-    put(hu, hu_out)
     homeward(0)
-    hidden_rows(last)
-    put(hh, hh_out)
 
     homeward(1)
     homeward(2)
@@ -1110,16 +1096,13 @@
         flat.append(jnp.concatenate(parts, axis=0))
     tok_flat = all_tok[...].reshape(ep * tok, dl)
     osg[...] = dot(flat[0], tok_flat)
-    put(osg, osg_out)
     osu[...] = dot(flat[1], tok_flat)
-    put(osu, osu_out)
     osd[...] = dot(flat[2], all_cot[...].reshape(ep * tok, dl))
-    put(osd, osd_out)
-
+
+    hidden_rows(last)
     for p in range(3, length):
         homeward(p)
     gtok[...] = shsum[...].astype(BF)
-    put(gtok, gtok_out)
     dg = jnp.concatenate([dgb[j] for j in range(ep)], axis=1)
     high = dg.astype(BF)
     low = (dg - high.astype(F32)).astype(BF)
@@ -1127,7 +1110,6 @@
     gw[...] = jnp.concatenate(
         [total[0:1, :tok], total[0:1, tok:], jnp.zeros((6, tok), F32)], axis=0
     )
-    put(gw, gw_out)
     for cond, c in sends:
         pl.when(cond)(c.wait_send)
     for b in range(3):
@@ -1141,30 +1123,10 @@
     left(share_t.at[1, :, :, any_tp], xy_s.at[0])
     left(back.at[pl.ds(0, ep - 1)], bk_s.at[0])
     left(dgb.at[pl.ds(0, ep - 1)], bk_s.at[1])
-    for c in outs:
-        c.wait()
 
 
 def grads_kernel(
     dims,
-    gtok_in,
-    gw_in,
-    osg_in,
-    osu_in,
-    osd_in,
-    stok_in,
-    scot_in,
-    hg_in,
-    hu_in,
-    hh_in,
-    gtok_out,
-    gw_out,
-    grad_gate,
-    grad_up,
-    grad_down,
-    osg_out,
-    osu_out,
-    osd_out,
     gtok,
     gw,
     osg,
@@ -1175,31 +1137,20 @@
     hg,
     hu,
     hh,
+    gtok_out,
+    gw_out,
+    grad_gate,
+    grad_up,
+    grad_down,
+    osg_out,
+    osu_out,
+    osd_out,
     gate_rows,
     up_rows,
     down_rows,
-    in_sem,
     out_sem,
 ):
     ne, chunks = dims
-    ins = []
-    for n, (src, dst) in enumerate(
-        (
-            (stok_in, stok),
-            (hg_in, hg),
-            (hu_in, hu),
-            (hh_in, hh),
-            (scot_in, scot),
-            (gtok_in, gtok),
-            (gw_in, gw),
-            (osg_in, osg),
-            (osu_in, osu),
-            (osd_in, osd),
-        )
-    ):
-        c = pltpu.make_async_copy(src, dst, in_sem.at[n])
-        c.start()
-        ins.append(c)
     outs = []
 
     def put(src, dst):
@@ -1207,24 +1158,6 @@
         c.start()
         outs.append(c)
 
-    def outer(a, b):
-        return lax.dot_general(a, b, (((0,), (0,)), ((), ())), preferred_element_type=F32)
-
-    def cut(size):
-        step = size // chunks
-        return [slice(i * step, (i + 1) * step) for i in range(chunks)]
-
-    for n in range(3):
-        ins[n].wait()
-    for e in range(ne):
-        for r in cut(stok.shape[2]):
-            left = stok[e, :, r]
-            gate_rows[e, r, :] = outer(left, hg[e])
-            put(gate_rows.at[e, r], grad_gate.at[e, r])
-            up_rows[e, r, :] = outer(left, hu[e])
-            put(up_rows.at[e, r], grad_up.at[e, r])
-    for n in range(3, 10):
-        ins[n].wait()
     for src, dst in (
         (gtok, gtok_out),
         (gw.at[pl.ds(0, gw_out.shape[0])], gw_out),
@@ -1233,6 +1166,21 @@
         (osd, osd_out),
     ):
         put(src, dst)
+
+    def outer(a, b):
+        return lax.dot_general(a, b, (((0,), (0,)), ((), ())), preferred_element_type=F32)
+
+    def cut(size):
+        step = size // chunks
+        return [slice(i * step, (i + 1) * step) for i in range(chunks)]
+
+    for e in range(ne):
+        for r in cut(stok.shape[2]):
+            left = stok[e, :, r]
+            gate_rows[e, r, :] = outer(left, hg[e])
+            put(gate_rows.at[e, r], grad_gate.at[e, r])
+            up_rows[e, r, :] = outer(left, hu[e])
+            put(up_rows.at[e, r], grad_up.at[e, r])
     for e in range(ne):
         for r in cut(hh.shape[2]):
             down_rows[e, r, :] = outer(hh[e, :, r], scot[e])
@@ -1268,6 +1216,7 @@
     dims = (ep, tp, tok, dl, ne, ff, sff, cap, rows, width, swidth, swid)
 
     hbm = pl.BlockSpec(memory_space=pltpu.HBM)
+    vmem = pl.BlockSpec(memory_space=pltpu.VMEM)
     dma = pltpu.SemaphoreType.DMA
     sds = jax.ShapeDtypeStruct
     shapes = (
@@ -1285,7 +1234,6 @@
     scratch = [
         pltpu.VMEM((top, tok), jnp.int32),
         pltpu.VMEM((top, tok), F32),
-        *[pltpu.VMEM(s.shape, s.dtype) for s in shapes],
         pltpu.VMEM((length, CORES, tok, dl), BF),
         pltpu.VMEM((length, CORES, tok, dl), BF),
         pltpu.VMEM((length, CORES, 8, tok), F32),
@@ -1313,7 +1261,6 @@
         pltpu.VMEM((tok, dl), F32),
         dma((6,)),
         dma((4,)),
-        dma((len(shapes),)),
         dma((6,)),
         dma((3 * length,)),
         dma((3 * length,)),
@@ -1329,25 +1276,31 @@
     ]
     outs = pl.pallas_call(
         functools.partial(line_kernel, dims),
-        out_shape=shapes,
+        out_shape=tuple([pltpu.VMEM(s.shape, s.dtype) for s in shapes]),
         in_specs=[hbm] * 10,
-        out_specs=tuple([hbm] * len(shapes)),
+        out_specs=tuple([vmem] * len(shapes)),
         scratch_shapes=scratch,
         compiler_params=pltpu.CompilerParams(
-            collective_id=0, has_side_effects=True, vmem_limit_bytes=60 * 1024 * 1024
+            collective_id=0, has_side_effects=True, vmem_limit_bytes=48 * 1024 * 1024
         ),
     )(
-        routes.T,
-        route_weights.T,
-        tokens,
-        cotangent,
-        expert_gate,
-        expert_up,
-        expert_down,
-        shared_gate,
-        shared_up,
-        shared_down,
+        *[
+            pltpu.with_memory_space_constraint(x, pltpu.HBM)
+            for x in (
+                routes.T,
+                route_weights.T,
+                tokens,
+                cotangent,
+                expert_gate,
+                expert_up,
+                expert_down,
+                shared_gate,
+                shared_up,
+                shared_down,
+            )
+        ]
     )
+    outs = [pltpu.with_memory_space_constraint(x, pltpu.VMEM) for x in outs]
     chunks = 4
     results = (
         sds((tok, dl), BF),
@@ -1362,15 +1315,13 @@
     gtok, gw, grad_gate, grad_up, grad_down, osg, osu, osd = pl.pallas_call(
         functools.partial(grads_kernel, (ne, chunks)),
         out_shape=results,
-        in_specs=[hbm] * len(shapes),
+        in_specs=[vmem] * len(shapes),
         out_specs=tuple([hbm] * len(results)),
         scratch_shapes=[
-            *[pltpu.VMEM(s.shape, s.dtype) for s in shapes],
             *[pltpu.VMEM(s.shape, s.dtype) for s in results[2:5]],
-            dma((len(shapes),)),
             dma((3 * ne * chunks + 5,)),
         ],
-        compiler_params=pltpu.CompilerParams(vmem_limit_bytes=60 * 1024 * 1024),
+        compiler_params=pltpu.CompilerParams(vmem_limit_bytes=24 * 1024 * 1024),
         name="grads",
     )(*outs)
     return gtok, gw.T, grad_gate, grad_up, grad_down, osg.T, osu.T, osd

time: 69.2 us -> 66.5 us (0.961)
  Pallas kernels: 68.3 us -> 65.5 us
    pallas_call x1, Pallas kernels: 6.81 us -> 5.11 us  [line_body(): pl.pallas_call(functools.partial(grads_kernel, (ne, chunks)), out_shape=r...]
    pallas_call x1, Pallas kernels: 61.4 us -> 60.4 us  [line_body(): pl.pallas_call(functools.partial(line_kernel, dims), out_shape=tuple([plt...]
where the time goes in v4:
time: 66.5 us; the launch traced here: 66.3 us
  Pallas kernels  65.5 us (98%)
  between operations  0.81 us (1%)
    pallas_call x1, Pallas kernels, line_body(): pl.pallas_call(functools.partial(line_kernel, dims), out_shape=tuple([plt...  60.4 us
    pallas_call x1, Pallas kernels, line_body(): pl.pallas_call(functools.partial(grads_kernel, (ne, chunks)), out_shape=r...  5.11 us

profile of v4, /device:TPU:0, one launch (start us, length us, event | category | flops | bytes accessed | tf_op | source)
XLA Modules:
  0.0 66.3 jit_solution(14447781601419294365)
XLA Ops:
  0.6 60.4 %shard_map.161 = (bf16[128,1024]{1,0:T(8,128)(2,1)S(1)}, f32[8,128]{1,0:T(8,128)S(1)}, f32[64,1024]{1,0:T(8,128)S(1)}, f32[64,1024]{1,0:T(8,128)S(1)}, f32[64,10...) custom-call(s32[2,128]{1,0:T(2,128)} %bitcast.5, ...), custom_call_target="tpu_custom_call" | custom-call | tf_op jit(solution)/shard_map/pallas_call | solution.py:1277
  61.1 5.1 %grads.1 = (bf16[128,1024]{1,0:T(8,128)(2,1)}, f32[2,128]{1,0:T(2,128)}, f32[2,1024,512]{2,1,0:T(8,128)}, f32[2,1024,512]{2,1,0:T(8,128)}, f32[2,512,1024]{2,1,0...) custom-call(bf16[128,1024]{1,0:T(8,128)(2,1)S(1)} %get-tuple-element.26.gtok, ...), custom_call_target="tpu_custom_call" | custom-call | tf_op jit(solution)/shard_map/grads/pallas_call | solution.py:1315

commit v5 on v4

--- a/solution.py
+++ b/solution.py
@@ -1167,6 +1167,9 @@
     ):
         put(src, dst)
 
+    def send(src, dst, n):
+        pltpu.make_async_copy(src, dst, out_sem.at[5 + n]).start()
+
     def outer(a, b):
         return lax.dot_general(a, b, (((0,), (0,)), ((), ())), preferred_element_type=F32)
 
@@ -1178,15 +1181,19 @@
         for r in cut(stok.shape[2]):
             left = stok[e, :, r]
             gate_rows[e, r, :] = outer(left, hg[e])
-            put(gate_rows.at[e, r], grad_gate.at[e, r])
+            send(gate_rows.at[e, r], grad_gate.at[e, r], 0)
             up_rows[e, r, :] = outer(left, hu[e])
-            put(up_rows.at[e, r], grad_up.at[e, r])
+            send(up_rows.at[e, r], grad_up.at[e, r], 1)
     for e in range(ne):
         for r in cut(hh.shape[2]):
             down_rows[e, r, :] = outer(hh[e, :, r], scot[e])
-            put(down_rows.at[e, r], grad_down.at[e, r])
+            send(down_rows.at[e, r], grad_down.at[e, r], 2)
     for c in outs:
         c.wait()
+    for n, (src, dst) in enumerate(
+        ((gate_rows, grad_gate), (up_rows, grad_up), (down_rows, grad_down))
+    ):
+        pltpu.make_async_copy(src, dst, out_sem.at[5 + n]).wait()
 
 
 def line_body(
@@ -1319,7 +1326,7 @@
         out_specs=tuple([hbm] * len(results)),
         scratch_shapes=[
             *[pltpu.VMEM(s.shape, s.dtype) for s in results[2:5]],
-            dma((3 * ne * chunks + 5,)),
+            dma((8,)),
         ],
         compiler_params=pltpu.CompilerParams(vmem_limit_bytes=24 * 1024 * 1024),
         name="grads",

time: 66.5 us -> 66.3 us (level)
  no operation moved by 1% of the time
where the time goes in v5:
time: 66.3 us; the launch traced here: 66.2 us
  Pallas kernels  65.3 us (98%)
  between operations  0.81 us (1%)
    pallas_call x1, Pallas kernels, line_body(): pl.pallas_call(functools.partial(line_kernel, dims), out_shape=tuple([plt...  60.4 us
    pallas_call x1, Pallas kernels, line_body(): pl.pallas_call(functools.partial(grads_kernel, (ne, chunks)), out_shape=r...  4.93 us

profile of v5, /device:TPU:0, one launch (start us, length us, event | category | flops | bytes accessed | tf_op | source)
XLA Modules:
  0.0 66.2 jit_solution(13804348551594765151)
XLA Ops:
  0.6 60.4 %shard_map.161 = (bf16[128,1024]{1,0:T(8,128)(2,1)S(1)}, f32[8,128]{1,0:T(8,128)S(1)}, f32[64,1024]{1,0:T(8,128)S(1)}, f32[64,1024]{1,0:T(8,128)S(1)}, f32[64,10...) custom-call(s32[2,128]{1,0:T(2,128)} %bitcast.5, ...), custom_call_target="tpu_custom_call" | custom-call | tf_op jit(solution)/shard_map/pallas_call | solution.py:1284
  61.1 4.9 %grads.1 = (bf16[128,1024]{1,0:T(8,128)(2,1)}, f32[2,128]{1,0:T(2,128)}, f32[2,1024,512]{2,1,0:T(8,128)}, f32[2,1024,512]{2,1,0:T(8,128)}, f32[2,512,1024]{2,1,0...) custom-call(bf16[128,1024]{1,0:T(8,128)(2,1)S(1)} %get-tuple-element.26.gtok, ...), custom_call_target="tpu_custom_call" | custom-call | tf_op jit(solution)/shard_map/grads/pallas_call | solution.py:1322
